TPU v7x, 32 devices: a whole 2x2x4 slice. The times are simulated.
32 devices in a mesh: fs: 8 (over z, y), tp: 4 (over x, core).
Axes of the slice: x: 2, y: 2, z: 4, core: 2. Of those that a mesh axis runs over, the one named last changes fastest.
Arguments:
- tokens: bfloat16 [2048, 2048], P('fs', 'tp'), may hold values from -12.1 to 12.1, as said below
- gate_weight: float32 [2048, 5632], P('fs', 'tp'), may hold values from -0.125 to 0.125
- up_weight: float32 [2048, 5632], P('fs', 'tp'), may hold values from -0.125 to 0.125
- down_weight: float32 [5632, 2048], P('tp', 'fs'), may hold values from -0.078125 to 0.078125
- gate_scale: float32 [4, 1408], P('tp', 'fs'), may hold values from 0.1 to 1.9
- up_scale: float32 [4, 1408], P('tp', 'fs'), may hold values from 0.1 to 1.9
- down_scale: float32 [4, 512], P('tp', 'fs'), may hold values from 0.16 to 4.6, as said below
- bgate_weight: float32 [2048, 2048], P('fs', 'tp'), may hold values from -0.125 to 0.125
- cgate_weight: float32 [2048, 2048], P('fs', 'tp'), may hold values from -0.125 to 0.125
- value_weight: float32 [2048, 2048], P('fs', 'tp'), may hold values from -0.125 to 0.125
- bgate_scale: float32 [4, 512], P('tp', 'fs'), may hold values from 0.1 to 1.9
- cgate_scale: float32 [4, 512], P('tp', 'fs'), may hold values from 0.1 to 1.9
- value_scale: float32 [4, 512], P('tp', 'fs'), may hold values from 0.1 to 1.9
- conv_taps: float32 [3, 2048], replicated, may hold values from -3.5 to 3.5
- mixout_weight: float32 [2048, 2048], P('tp', 'fs'), may hold values from -0.125 to 0.125
- mixout_scale: float32 [4, 512], P('tp', 'fs'), may hold values from 0.16 to 4.6, as said below
- first_gain: float32 [2048], replicated, may hold values from 0.1 to 1.9
- first_shift: float32 [2048], replicated, may hold values from -1.8 to 1.8
- mixer_gain: float32 [2048], replicated, may hold values from 0.1 to 1.9
- mixer_shift: float32 [2048], replicated, may hold values from -1.8 to 1.8
- last_gain: float32 [2048], replicated, may hold values from 0.1 to 1.9
- last_shift: float32 [2048], replicated, may hold values from -1.8 to 1.8
Outputs:
- layer_out: bfloat16 [2048, 2048], P('fs', 'tp')
Inputs may be any that keep to these rules, and one draw needn't show every extreme that they name: `tokens`: normal values times one factor for each of 4 equal consecutive blocks of the features. `down_scale`: positive; one factor for each row times a spread over the columns. `mixout_scale`: positive; one factor for each row times a spread over the columns.
All inputs are finite; a program needn't handle non-finite values.
Results may differ from a plain program's by a relative error of at most 0.025.
Values may be sent and summed in bfloat16 or wider, within the bound.
A program may use at most 64 MiB of HBM per device.

v0:
```python
import jax
import jax.numpy as jnp
from jax import lax
from jax.sharding import PartitionSpec as P

TAPS = 3
LENGTH = 128


RESIDUAL_SCALE = 1.4142135623730951
HALF_STEP = 0.5
EPSILON = 1e-05


def add_rows(gathered, shard_piece):
    return jnp.dot(gathered, shard_piece, preferred_element_type=jnp.float32)


def features(inputs):
    return lax.all_gather(inputs, "tp", axis=1, tiled=True)


def post_norm(residual, branch, norm_gain, norm_shift):
    summed = RESIDUAL_SCALE * residual.astype(jnp.float32) + branch
    moments = lax.psum((jnp.sum(summed, -1), jnp.sum(summed * summed, -1)), "tp")
    feature_total = summed.shape[1] * lax.axis_size("tp")
    average = (moments[0] / feature_total)[:, None]
    mean_square = (moments[1] / feature_total)[:, None]
    variance = mean_square - average * average
    return ((summed - average) * lax.rsqrt(variance + EPSILON) * norm_gain + norm_shift).astype(
        jnp.bfloat16
    )


def spread_back(weight_cols, left_rows):
    return (
        lax.psum_scatter(
            lax.dot_general(
                weight_cols, left_rows, (((0,), (1,)), ((), ())), preferred_element_type=jnp.float32
            ).astype(jnp.bfloat16),
            "tp",
            scatter_dimension=0,
            tiled=True,
        )
        .astype(jnp.float32)
        .T
    )


def shards(
    tokens,
    gate_weight,
    up_weight,
    down_weight,
    gate_scale,
    up_scale,
    down_scale,
    bgate_weight,
    cgate_weight,
    value_weight,
    bgate_scale,
    cgate_scale,
    value_scale,
    conv_taps,
    mixout_weight,
    mixout_scale,
    first_gain,
    first_shift,
    mixer_gain,
    mixer_shift,
    last_gain,
    last_shift,
):
    scales = (
        lax.all_gather(gate_scale, "fs", axis=1, tiled=True),
        lax.all_gather(up_scale, "fs", axis=1, tiled=True),
        lax.all_gather(down_scale, "fs", axis=1, tiled=True),
        lax.all_gather(bgate_scale, "fs", axis=1, tiled=True),
        lax.all_gather(cgate_scale, "fs", axis=1, tiled=True),
        lax.all_gather(value_scale, "fs", axis=1, tiled=True),
        lax.all_gather(mixout_scale, "fs", axis=1, tiled=True),
    )
    gate_cols, up_cols, down_cols, bgate_cols, cgate_cols, value_cols, mixout_cols = [
        scale_row.reshape(-1) for scale_row in scales
    ]
    tp_index = lax.axis_index("tp")
    columns = tokens.shape[1]

    def own_part(vector):
        return lax.dynamic_slice_in_dim(vector, tp_index * columns, columns)

    gate_low = gate_weight.astype(jnp.bfloat16)
    up_low = up_weight.astype(jnp.bfloat16)
    down_low = down_weight.astype(jnp.bfloat16)
    kept_gate, kept_up = (
        lax.all_gather(gate_low, "fs", axis=0, tiled=True),
        lax.all_gather(up_low, "fs", axis=0, tiled=True),
    )
    kept_down = lax.all_gather(down_low, "fs", axis=1, tiled=True)

    def channel_mix(gathered):
        gate_sum = jnp.dot(gathered, kept_gate, preferred_element_type=jnp.float32)
        up_sum = jnp.dot(gathered, kept_up, preferred_element_type=jnp.float32)
        hidden = (jax.nn.silu(gate_sum * gate_cols) * (up_sum * up_cols)).astype(jnp.bfloat16)
        return HALF_STEP * (spread_back(kept_down, hidden) * down_cols)

    first = post_norm(
        tokens, channel_mix(features(tokens)), own_part(first_gain), own_part(first_shift)
    )
    gathered = features(first)
    bgate_low = bgate_weight.astype(jnp.bfloat16)
    channels = bgate_low.shape[1]
    outgate = add_rows(gathered, lax.all_gather(bgate_low, "fs", axis=0, tiled=True))
    ingate = add_rows(
        gathered, lax.all_gather(cgate_weight.astype(jnp.bfloat16), "fs", axis=0, tiled=True)
    )
    values = add_rows(
        gathered, lax.all_gather(value_weight.astype(jnp.bfloat16), "fs", axis=0, tiled=True)
    )
    tap_weights = lax.dynamic_slice_in_dim(conv_taps, tp_index * channels, channels, 1)
    mixed = (ingate * cgate_cols * (values * value_cols)).reshape(-1, LENGTH, channels)
    padded = jnp.pad(mixed, ((0, 0), (TAPS - 1, 0), (0, 0)))
    convolved = jnp.zeros(mixed.shape, jnp.float32)
    for tap_index in range(TAPS):
        convolved = convolved + tap_weights[tap_index] * padded[:, tap_index : tap_index + LENGTH]
    gated = (outgate * bgate_cols * convolved.reshape(-1, channels)).astype(jnp.bfloat16)
    mix_full = lax.all_gather(mixout_weight.astype(jnp.bfloat16), "fs", axis=1, tiled=True)
    second = post_norm(
        first,
        spread_back(mix_full, gated) * mixout_cols,
        own_part(mixer_gain),
        own_part(mixer_shift),
    )
    return post_norm(
        second, channel_mix(features(second)), own_part(last_gain), own_part(last_shift)
    )


def solution(mesh):
    in_specs = (
        P("fs", "tp"),
        P("fs", "tp"),
        P("fs", "tp"),
        P("tp", "fs"),
        P("tp", "fs"),
        P("tp", "fs"),
        P("tp", "fs"),
        P("fs", "tp"),
        P("fs", "tp"),
        P("fs", "tp"),
        P("tp", "fs"),
        P("tp", "fs"),
        P("tp", "fs"),
        P(),
        P("tp", "fs"),
        P("tp", "fs"),
        P(),
        P(),
        P(),
        P(),
        P(),
        P(),
    )
    out_specs = P("fs", "tp")
    return jax.shard_map(shards, mesh=mesh, in_specs=in_specs, out_specs=out_specs, check_vma=False)
```

profile of v0, /device:TPU:0, one launch (start us, length us, event | category | flops | bytes accessed | tf_op | source)
XLA Modules:
  0.0 669.1 jit_solution(10766681198082173955)
XLA Ops:
  6.5 0.7 all-gather.11.cloned.1.call-update
  7.3 2.3 convert_element_type.78
  9.7 0.9 convert_element_type.79
  10.8 0.5 copy-done.5
  11.2 0.9 convert_element_type.81
  12.3 0.6 dynamic-slice
  14.2 0.3 dynamic-update-slice
  14.5 0.3 dynamic-update-slice.1
  15.2 39.5 %all-reduce.8 = (f32[1408]{0:T(1024)S(1)}, f32[1408]{0:T(1024)S(1)}, f32[512]{0:T(512)S(1)}, f32[512]{0:T(512)S(1)}, f32[512]{0:T(512)S(1)}, /*index=5*/f32[512]{0:T(512)S(1)}, f32[512]{0:T(512)S(1)}) all-reduce(f32[1408]{0:T(1024)S(1)} %dynamic-update-slice, f32[1408]{0:T(1024)S(1)} %dynamic-update-slice.1, ...), channel_id=1, replica_groups=mesh['fs'=8,'tp'=4] {'fs'}, use_global_device_ids=true, to_apply=%add.1 | all-reduce | flops 5376 | bytes 43008
  54.7 68.3 %all-gather.13.cloned.1.call-done = bf16[2048,1408]{1,0:T(8,128)(2,1)} async-done(((bf16[256,1408]{1,0:T(8,128)(2,1)}), bf16[2048,1408]{1,0:T(8,128)(2,1)}) %all-gather.13.cloned.1.call-update) | async-done | bytes 5767184 | tf_op jit(solution)/shard_map/all_gather | solution.py:96
  123.1 4.8 convolution_multiply_fusion.3
  127.9 87.9 %all-gather.15.cloned.1.call-done = bf16[2048,1408]{1,0:T(8,128)(2,1)} async-done(((bf16[256,1408]{1,0:T(8,128)(2,1)}), bf16[2048,1408]{1,0:T(8,128)(2,1)}) %all-gather.15.cloned.1.call-update) | async-done | bytes 5767184 | tf_op jit(solution)/shard_map/all_gather | solution.py:97
  215.8 93.2 %all-gather.17.cloned.1.call-done = bf16[1408,2048]{1,0:T(8,128)(2,1)} async-done(((bf16[1408,256]{1,0:T(8,128)(2,1)}), bf16[1408,2048]{1,0:T(8,128)(2,1)}) %all-gather.17.cloned.1.call-update) | async-done | bytes 5767184 | tf_op jit(solution)/shard_map/all_gather | solution.py:99
  309.0 9.0 %fusion.4 = bf16[2048,256]{0,1:T(8,128)(2,1)} fusion(bf16[1408,2048]{1,0:T(8,128)(2,1)} %all-gather.17.cloned.1.call-done, bf16[256,2048]{1,0:T(8,128)(2,1)S(1)} %copy-done.12, bf16[2048,1408]{1,0:T(8,128)(2,1)} %all-gather.15.cloned.1.call-done, f32[256,1408]{1,0:T(8,128)S(1)} %convolution_multiply_fusion.3, f32[1408]{0:T(1024)S(1)} %get-tuple-element.12), kind=kOutput, calls=%fused_computation.11 | convolution fusion | flops 2955837440 | bytes 15078912 | tf_op jit(solution)/shard_map/dot_general | solution.py:38
  318.1 0.7 convert_element_type.88
  318.9 0.8 dynamic_slice.21
  319.7 0.8 dynamic_slice.22
  320.5 20.6 %reduce-scatter.4.cloned.1.call-done = bf16[512,256]{0,1:T(8,128)(2,1)} async-done(((bf16[2048,256]{0,1:T(8,128)(2,1)}), bf16[512,256]{0,1:T(8,128)(2,1)}) %reduce-scatter.4.cloned.1.call-update) | async-done | bytes 262160 | tf_op jit(solution)/shard_map/reduce_scatter | solution.py:37
  341.1 1.2 fusion.15
  342.3 5.8 all-reduce.11
  348.1 1.9 add_convert_fusion.2
  350.0 0.7 convert_element_type.89
  350.8 0.7 convert_element_type.87
  351.7 0.7 convert_element_type.91
  352.5 0.9 constant_dynamic-slice_fusion
  353.4 38.9 %all-gather.23.cloned.1.call-done = bf16[2048,512]{1,0:T(8,128)(2,1)} async-done(((bf16[256,512]{1,0:T(8,128)(2,1)}), bf16[2048,512]{1,0:T(8,128)(2,1)}) %all-gather.23.cloned.1.call-update) | async-done | bytes 2097168 | tf_op jit(solution)/shard_map/all_gather | solution.py:115
  392.2 16.8 %all-gather.19.cloned.1.call-done = bf16[256,2048]{1,0:T(8,128)(2,1)} async-done(((bf16[256,512]{1,0:T(8,128)(2,1)}), bf16[256,2048]{1,0:T(8,128)(2,1)}) %all-gather.19.cloned.1.call-update) | async-done | bytes 1048592 | tf_op jit(solution)/shard_map/all_gather | solution.py:20
  409.0 2.7 convolution_multiply_fusion.5
  411.8 48.5 %all-gather.25.cloned.1.call-done = bf16[2048,512]{1,0:T(8,128)(2,1)} async-done(((bf16[256,512]{1,0:T(8,128)(2,1)}), bf16[2048,512]{1,0:T(8,128)(2,1)}) %all-gather.25.cloned.1.call-update) | async-done | bytes 2097168 | tf_op jit(solution)/shard_map/all_gather | solution.py:118
  460.3 2.3 fusion.7
  462.8 47.3 %all-gather.21.cloned.1.call-done = bf16[2048,512]{1,0:T(8,128)(2,1)} async-done(((bf16[256,512]{1,0:T(8,128)(2,1)}), bf16[2048,512]{1,0:T(8,128)(2,1)}) %all-gather.21.cloned.1.call-update) | async-done | bytes 2097168 | tf_op jit(solution)/shard_map/all_gather | solution.py:113
  510.1 50.8 %all-gather.27.cloned.1.call-done = bf16[512,2048]{1,0:T(8,128)(2,1)} async-done(((bf16[512,256]{1,0:T(8,128)(2,1)}), bf16[512,2048]{1,0:T(8,128)(2,1)}) %all-gather.27.cloned.1.call-update) | async-done | bytes 2097168 | tf_op jit(solution)/shard_map/all_gather | solution.py:127
  560.9 4.7 fusion.6
  565.6 0.8 dynamic_slice.24
  566.4 0.8 dynamic_slice.25
  567.1 21.6 %reduce-scatter.6.cloned.1.call-done = bf16[512,256]{0,1:T(8,128)(2,1)} async-done(((bf16[2048,256]{0,1:T(8,128)(2,1)}), bf16[512,256]{0,1:T(8,128)(2,1)}) %reduce-scatter.6.cloned.1.call-update) | async-done | bytes 262160 | tf_op jit(solution)/shard_map/reduce_scatter | solution.py:37
  588.7 1.2 fusion.14
  589.9 5.8 all-reduce.10
  595.6 1.8 add_convert_fusion.1
  597.7 17.2 %all-gather.29.cloned.1.call-done = bf16[256,2048]{1,0:T(8,128)(2,1)} async-done(((bf16[256,512]{1,0:T(8,128)(2,1)}), bf16[256,2048]{1,0:T(8,128)(2,1)}) %all-gather.29.cloned.1.call-update) | async-done | bytes 1048592 | tf_op jit(solution)/shard_map/all_gather | solution.py:20
  615.0 4.8 convolution_multiply_fusion.1
  619.8 9.0 %fusion.5 = bf16[2048,256]{0,1:T(8,128)(2,1)} fusion(bf16[1408,2048]{1,0:T(8,128)(2,1)} %all-gather.17.cloned.1.call-done, bf16[256,2048]{1,0:T(8,128)(2,1)S(1)} %copy-done.13, bf16[2048,1408]{1,0:T(8,128)(2,1)} %all-gather.15.cloned.1.call-done, f32[256,1408]{1,0:T(8,128)S(1)} %convolution_multiply_fusion.1, f32[1408]{0:T(1024)S(1)} %get-tuple-element.12), kind=kOutput, calls=%fused_computation.12 | convolution fusion | flops 2955837440 | bytes 15078912 | tf_op jit(solution)/shard_map/dot_general | solution.py:38
  628.8 0.8 dynamic_slice.26
  629.6 0.8 dynamic_slice.27
  630.4 23.4 %reduce-scatter.8.cloned.1.call-done = bf16[512,256]{0,1:T(8,128)(2,1)} async-done(((bf16[2048,256]{0,1:T(8,128)(2,1)}), bf16[512,256]{0,1:T(8,128)(2,1)}) %reduce-scatter.8.cloned.1.call-update) | async-done | bytes 262160 | tf_op jit(solution)/shard_map/reduce_scatter | solution.py:37
  653.8 1.2 fusion.16
  655.0 5.8 all-reduce.9
  660.7 1.9 add_convert_fusion
  (81 shorter events, 1.6 us)
Async XLA Ops:
  6.5 3.2 copy-start.4
  6.5 48.2 %all-gather.11.cloned.1.call-start = ((), (), s32[]{:S(2)}) async-start(), calls=%async_computation.3 | async-start | bytes 1310720 | tf_op jit(solution)/shard_map/all_gather | solution.py:20
  7.3 115.8 %all-gather.13.cloned.1.call-start = ((), (), s32[]{:S(2)}) async-start(), calls=%async_computation.4 | async-start | bytes 6488064 | tf_op jit(solution)/shard_map/all_gather | solution.py:96
  9.6 1.6 copy-start.5
  9.6 206.1 %all-gather.15.cloned.1.call-start = ((), (), s32[]{:S(2)}) async-start(), calls=%async_computation.5 | async-start | bytes 6488064 | tf_op jit(solution)/shard_map/all_gather | solution.py:97
  10.7 1.6 copy-start.19
  10.7 3.5 copy-start.10
  10.7 3.8 copy-start.11
  10.7 4.1 copy-start.14
  10.7 4.2 copy-start.15
  10.7 4.3 copy-start.16
  10.7 4.3 copy-start.17
  10.7 4.4 copy-start.18
  10.7 298.3 %all-gather.17.cloned.1.call-start = ((), (), s32[]{:S(2)}) async-start(), calls=%async_computation.6 | async-start | bytes 6488064 | tf_op jit(solution)/shard_map/all_gather | solution.py:99
  12.2 328.9 %reduce-scatter.4.cloned.1.call-start = ((), (), s32[]{:S(2)}) async-start(), calls=%async_computation.7 | async-start | bytes 1310720 | tf_op jit(solution)/shard_map/reduce_scatter | solution.py:37
  123.0 186.0 %copy-start.12 = (bf16[256,2048]{1,0:T(8,128)(2,1)S(1)}, bf16[256,2048]{1,0:T(8,128)(2,1)}, u32[]{:S(2)}) copy-start(bf16[256,2048]{1,0:T(8,128)(2,1)} %all-gather.11.cloned.1.call-done) | copy-start | bytes 3145732
  309.0 9.1 %copy-start.6 = (f32[256,512]{1,0:T(8,128)S(1)}, f32[256,512]{1,0:T(8,128)}, u32[]{:S(2)}) copy-start(f32[256,512]{1,0:T(8,128)} %param.30) | copy-start | bytes 1572868
  318.0 23.1 %copy-start.3 = (bf16[256,512]{1,0:T(8,128)(2,1)S(1)}, bf16[256,512]{1,0:T(8,128)(2,1)}, u32[]{:S(2)}) copy-start(bf16[256,512]{1,0:T(8,128)(2,1)} %param.22) | copy-start | bytes 786436
  318.0 32.0 %copy-start.7 = (f32[256,512]{1,0:T(8,128)S(1)}, f32[256,512]{1,0:T(8,128)}, u32[]{:S(2)}) copy-start(f32[256,512]{1,0:T(8,128)} %param.31) | copy-start | bytes 1572868
  318.0 32.8 %copy-start.8 = (f32[256,512]{1,0:T(8,128)S(1)}, f32[256,512]{1,0:T(8,128)}, u32[]{:S(2)}) copy-start(f32[256,512]{1,0:T(8,128)} %param.29) | copy-start | bytes 1572868
  318.0 74.2 %all-gather.23.cloned.1.call-start = ((), (), s32[]{:S(2)}) async-start(), calls=%async_computation.10 | async-start | bytes 2359296 | tf_op jit(solution)/shard_map/all_gather | solution.py:115
  318.8 32.8 %copy-start.9 = (f32[512,256]{1,0:T(8,128)S(1)}, f32[512,256]{1,0:T(8,128)}, u32[]{:S(2)}) copy-start(f32[512,256]{1,0:T(8,128)} %param.36) | copy-start | bytes 1572868
  318.8 90.2 %all-gather.19.cloned.1.call-start = ((), (), s32[]{:S(2)}) async-start(), calls=%async_computation.8 | async-start | bytes 1310720 | tf_op jit(solution)/shard_map/all_gather | solution.py:20
  350.0 110.3 %all-gather.25.cloned.1.call-start = ((), (), s32[]{:S(2)}) async-start(), calls=%async_computation.11 | async-start | bytes 2359296 | tf_op jit(solution)/shard_map/all_gather | solution.py:118
  350.8 159.3 %all-gather.21.cloned.1.call-start = ((), (), s32[]{:S(2)}) async-start(), calls=%async_computation.9 | async-start | bytes 2359296 | tf_op jit(solution)/shard_map/all_gather | solution.py:113
  351.6 209.3 %all-gather.27.cloned.1.call-start = ((), (), s32[]{:S(2)}) async-start(), calls=%async_computation.12 | async-start | bytes 2359296 | tf_op jit(solution)/shard_map/all_gather | solution.py:127
  352.4 236.3 %reduce-scatter.6.cloned.1.call-start = ((), (), s32[]{:S(2)}) async-start(), calls=%async_computation.13 | async-start | bytes 1310720 | tf_op jit(solution)/shard_map/reduce_scatter | solution.py:37
  409.0 51.2 %copy-start = (bf16[256,2048]{1,0:T(8,128)(2,1)S(1)}, bf16[256,2048]{1,0:T(8,128)(2,1)}, u32[]{:S(2)}) copy-start(bf16[256,2048]{1,0:T(8,128)(2,1)} %all-gather.19.cloned.1.call-done) | copy-start | bytes 3145732
  560.9 27.8 %copy-start.1 = (bf16[256,512]{1,0:T(8,128)(2,1)S(1)}, bf16[256,512]{1,0:T(8,128)(2,1)}, u32[]{:S(2)}) copy-start(bf16[256,512]{1,0:T(8,128)(2,1)} %add_convert_fusion.2) | copy-start | bytes 786436
  565.6 49.4 %all-gather.29.cloned.1.call-start = ((), (), s32[]{:S(2)}) async-start(), calls=%async_computation.14 | async-start | bytes 1310720 | tf_op jit(solution)/shard_map/all_gather | solution.py:20
  597.5 56.3 %reduce-scatter.8.cloned.1.call-start = ((), (), s32[]{:S(2)}) async-start(), calls=%async_computation.15 | async-start | bytes 1310720 | tf_op jit(solution)/shard_map/reduce_scatter | solution.py:37
  615.0 4.8 copy-start.13
  619.8 34.0 %copy-start.2 = (bf16[256,512]{1,0:T(8,128)(2,1)S(1)}, bf16[256,512]{1,0:T(8,128)(2,1)}, u32[]{:S(2)}) copy-start(bf16[256,512]{1,0:T(8,128)(2,1)} %add_convert_fusion.1) | copy-start | bytes 786436
Sparse Core Ops, SparseCore 0:
  8.9 19.4 all-gather.10
  30.5 92.4 all-gather.12
  125.2 90.4 all-gather.14
  217.7 91.2 all-gather.16
  318.1 22.9 reduce-scatter.3
  343.1 49.1 all-gather.22
  393.8 15.2 all-gather.18
  411.2 49.0 all-gather.24
  462.4 47.6 all-gather.20
  512.0 48.8 all-gather.26
  565.7 22.9 reduce-scatter.5
  597.6 17.3 all-gather.28
  629.0 24.7 reduce-scatter.7
where the time goes:
time: 670 us; the launch traced here: 669 us
  waiting for transfers between devices  536 us (80%)
  blocking collectives  56.8 us (8%)
  matrix products  37.3 us (6%)
  other arithmetic  16.5 us (2%)
  between operations  14.8 us (2%)
  local copies, waits for them, and re-layouts  7.65 us (1%)
    all_gather x1, waiting for transfers between devices, shards(): kept_down = lax.all_gather(down_low, 'fs', axis=1, tiled=True)  93.2 us
    all_gather x1, waiting for transfers between devices, shards(): lax.all_gather(up_low, 'fs', axis=0, tiled=True)  87.9 us
    all_gather x1, waiting for transfers between devices, shards(): lax.all_gather(gate_low, 'fs', axis=0, tiled=True)  68.3 us
    reduce_scatter x3, waiting for transfers between devices, spread_back(): lax.psum_scatter(lax.dot_general(weight_cols, left_rows, (((0,), (1,)), (...  65.6 us
    all_gather x1, waiting for transfers between devices, shards(): lax.all_gather(mixout_weight.astype(jnp.bfloat16), 'fs', axis=1, tiled=True)  50.8 us
    all_gather x1, waiting for transfers between devices, shards(): lax.all_gather(value_weight.astype(jnp.bfloat16), 'fs', axis=0, tiled=True)  48.5 us
    all_gather x1, waiting for transfers between devices, shards(): lax.all_gather(bgate_low, 'fs', axis=0, tiled=True)  47.3 us
    unnamed x1, blocking collectives  39.5 us
  transfers between devices with their start and end apart: 13, of which 12 were waited for; matrix products, arithmetic and copies ran while one was open for 4% of the time, Pallas kernels for 0%

commit v1 on v0

--- a/solution.py
+++ b/solution.py
@@ -1,15 +1,338 @@
+import functools
+
 import jax
 import jax.numpy as jnp
 from jax import lax
+from jax.experimental import pallas as pl
+from jax.experimental.pallas import tpu as pltpu
+from jax.sharding import Mesh
 from jax.sharding import PartitionSpec as P
 
 TAPS = 3
 LENGTH = 128
-
+CORES = 2
 
 RESIDUAL_SCALE = 1.4142135623730951
 HALF_STEP = 0.5
 EPSILON = 1e-05
+BY_AXIS = pl.DeviceIdType.MESH
+ANY = pl.BlockSpec(memory_space=pl.ANY)
+VMEM = pl.BlockSpec(memory_space=pltpu.VMEM)
+
+
+def greet(depth, axes):
+    barrier = pltpu.get_barrier_semaphore()
+    z = lax.axis_index("z")
+    targets = [{"z": lax.rem(z + d, depth)} for d in range(1, depth)]
+    targets += [{axis: 1 - lax.axis_index(axis)} for axis in axes]
+    for target in targets:
+        pl.semaphore_signal(barrier, inc=1, device_id=target, device_id_type=BY_AXIS)
+    pl.semaphore_wait(barrier, len(targets))
+
+
+def remote(src, dst, send, recv, target):
+    return pltpu.make_async_remote_copy(
+        src_ref=src, dst_ref=dst, send_sem=send, recv_sem=recv, device_id=target, device_id_type=BY_AXIS
+    )
+
+
+def start_gather(depth, own, whole, z, c, sems):
+    zsend, zrecv, csend, crecv, local = sems
+    keep = pltpu.make_async_copy(own, whole.at[z, c], local)
+    keep.start()
+    across = []
+    for d in range(1, depth):
+        copy = remote(own, whole.at[z, c], zsend.at[d], zrecv.at[d], {"z": lax.rem(z + d, depth)})
+        copy.start()
+        across.append(copy)
+    beside = [remote(own, whole.at[z, c], csend.at[0], crecv.at[0], {"c": 1 - c})]
+    beside[0].start()
+    return keep, across, beside
+
+
+def end_gather(depth, whole, z, c, sems, state):
+    zsend, zrecv, csend, crecv, local = sems
+    keep, across, beside = state
+    for d in range(1, depth):
+        across[d - 1].wait_recv()
+        place = whole.at[lax.rem(z - d + depth, depth), c]
+        copy = remote(place, place, csend.at[d], crecv.at[d], {"c": 1 - c})
+        copy.start()
+        beside.append(copy)
+    for copy in beside:
+        copy.wait()
+    for copy in across:
+        copy.wait_send()
+    keep.wait()
+
+
+def weights_kernel(
+    depth, w_ref, s_ref, t_ref, g_ref, sa_ref, ta_ref,
+    zsend, zrecv, ysend, yrecv, xsend, xrecv, dsend, drecv,
+    ssend, srecv, tzsend, tzrecv, tcsend, tcrecv, local,
+):
+    z, y, x, c = (lax.axis_index(axis) for axis in ("z", "y", "x", "c"))
+    width = w_ref.shape[2]
+    greet(depth, ("y", "x", "c"))
+
+    def place(px, pz, py):
+        start = pl.multiple_of((pz * 2 + py) * width, width)
+        return g_ref.at[px, :, pl.ds(start, width)]
+
+    to_x, to_y, to_c = {"x": 1 - x}, {"y": 1 - y}, {"c": 1 - c}
+    own_scale = pltpu.make_async_copy(s_ref, sa_ref.at[c, x, y, z], local.at[0])
+    own_scale.start()
+    scale_sends = []
+    for d in range(1, depth):
+        copy = remote(s_ref, sa_ref.at[c, x, y, z], ssend.at[d], srecv.at[d], {"z": lax.rem(z + d, depth)})
+        copy.start()
+        scale_sends.append(copy)
+    token_sems = (tzsend, tzrecv, tcsend, tcrecv, local.at[1])
+    token_state = start_gather(depth, t_ref, ta_ref, z, c, token_sems)
+    z_copies = []
+    for d in range(1, depth):
+        target = lax.rem(z + d, depth)
+        copy = remote(w_ref.at[target], place(x, z, y), zsend.at[d], zrecv.at[d], {"z": target})
+        copy.start()
+        z_copies.append(copy)
+    keep = pltpu.make_async_copy(w_ref.at[z], place(x, z, y), local.at[2])
+    keep.start()
+
+    y_copies, x_copies, d_copies = [], [], []
+
+    def relay(d):
+        source = lax.rem(z - d + depth, depth)
+        if d % 2 == 0:
+            y_copies[d].wait_recv()
+            block = place(x, source, 1 - y)
+            copy = remote(block, block, dsend.at[d], drecv.at[d], to_x)
+        else:
+            x_copies[d].wait_recv()
+            block = place(1 - x, source, y)
+            copy = remote(block, block, dsend.at[d], drecv.at[d], to_y)
+        copy.start()
+        d_copies.append(copy)
+
+    for d in range(depth):
+        source = lax.rem(z - d + depth, depth)
+        block = place(x, source, y)
+        origin = w_ref.at[z] if d == 0 else block
+        if d > 0:
+            z_copies[d - 1].wait_recv()
+        ycopy = remote(origin, block, ysend.at[d], yrecv.at[d], to_y)
+        xcopy = remote(origin, block, xsend.at[d], xrecv.at[d], to_x)
+        ycopy.start()
+        xcopy.start()
+        y_copies.append(ycopy)
+        x_copies.append(xcopy)
+        if d > 0:
+            relay(d - 1)
+        if d == 0:
+            own_scale.wait()
+            for copy in scale_sends:
+                copy.wait()
+            column = sa_ref.at[c, x, y]
+            hop = remote(column, column, ssend.at[0], srecv.at[0], to_y)
+            hop.start()
+            hop.wait()
+            plane = sa_ref.at[c, x]
+            hop = remote(plane, plane, ssend.at[depth], srecv.at[depth], to_x)
+            hop.start()
+            hop.wait()
+            half = sa_ref.at[c]
+            hop = remote(half, half, ssend.at[depth + 1], srecv.at[depth + 1], to_c)
+            hop.start()
+            hop.wait()
+            end_gather(depth, ta_ref, z, c, token_sems, token_state)
+    relay(depth - 1)
+    for d in range(depth):
+        if d % 2 == 0:
+            x_copies[d].wait_recv()
+        else:
+            y_copies[d].wait_recv()
+        d_copies[d].wait_recv()
+        y_copies[d].wait_send()
+        x_copies[d].wait_send()
+        d_copies[d].wait_send()
+    for copy in z_copies:
+        copy.wait_send()
+    keep.wait()
+
+
+def spread_weights(depth, blocks, scale_block, own_rows):
+    rows, width = blocks.shape[1:]
+    dma = pltpu.SemaphoreType.DMA
+    return pl.pallas_call(
+        functools.partial(weights_kernel, depth),
+        out_shape=(
+            jax.ShapeDtypeStruct((2, rows, depth * 2 * width), jnp.bfloat16),
+            jax.ShapeDtypeStruct((CORES, 2, 2, depth) + scale_block.shape, jnp.float32),
+            jax.ShapeDtypeStruct((depth, CORES) + own_rows.shape, jnp.bfloat16),
+        ),
+        in_specs=[ANY, ANY, ANY],
+        out_specs=(ANY, ANY, ANY),
+        scratch_shapes=[dma((depth,)) for _ in range(8)]
+        + [dma((depth + 2,)), dma((depth + 2,))]
+        + [dma((depth,)) for _ in range(4)]
+        + [dma((3,))],
+        compiler_params=pltpu.CompilerParams(collective_id=0, has_side_effects=True),
+        name="spread_weights",
+    )(blocks, scale_block, own_rows)
+
+
+def join_kernel(depth, gather, part_ref, res_ref, scale_ref, gain_ref, shift_ref, out_ref, *rest):
+    if gather:
+        ta_ref, rest = rest[0], rest[1:]
+    half, sums, got, hsend, hrecv, rsend, rrecv = rest[:7]
+    z, c = lax.axis_index("z"), lax.axis_index("c")
+    greet(depth, ("c",))
+    order = list(range(1, depth)) + [0]
+    halves = {}
+    for d in order:
+        target = lax.rem(z + d, depth)
+        halves[d] = remote(part_ref.at[target, 1 - c], half.at[d], hsend.at[d], hrecv.at[d], {"c": 1 - c})
+        halves[d].start()
+    shares = []
+    for d in order[:-1]:
+        target = lax.rem(z + d, depth)
+        halves[d].wait_recv()
+        both = part_ref[target, c].astype(jnp.float32) + half[d].astype(jnp.float32)
+        sums[d] = both.astype(jnp.bfloat16)
+        copy = remote(sums.at[d], got.at[d], rsend.at[d], rrecv.at[d], {"z": target})
+        copy.start()
+        shares.append(copy)
+    halves[0].wait_recv()
+    total = part_ref[z, c].astype(jnp.float32) + half[0].astype(jnp.float32)
+    for d in range(1, depth):
+        shares[d - 1].wait_recv()
+        total = total + got[d].astype(jnp.float32)
+    summed = RESIDUAL_SCALE * res_ref[...].astype(jnp.float32) + total * scale_ref[...]
+    count = summed.shape[1]
+    average = jnp.sum(summed, -1, keepdims=True) / count
+    mean_square = jnp.sum(summed * summed, -1, keepdims=True) / count
+    variance = mean_square - average * average
+    normed = (summed - average) * lax.rsqrt(variance + EPSILON) * gain_ref[...] + shift_ref[...]
+    out_ref[...] = normed.astype(jnp.bfloat16)
+    if gather:
+        sems = rest[7:]
+        state = start_gather(depth, out_ref, ta_ref, z, c, sems)
+        end_gather(depth, ta_ref, z, c, sems, state)
+    for d in range(depth):
+        halves[d].wait_send()
+    for copy in shares:
+        copy.wait_send()
+
+
+def join(depth, gather, number, part, residual, scale, gain, shift):
+    rows, features = residual.shape
+    dma = pltpu.SemaphoreType.DMA
+    block = pltpu.VMEM((depth, rows, features), jnp.bfloat16)
+    out_shape = [jax.ShapeDtypeStruct((rows, features), jnp.bfloat16)]
+    out_specs = [VMEM]
+    scratch = [block, block, block] + [dma((depth,)) for _ in range(4)]
+    if gather:
+        out_shape.append(jax.ShapeDtypeStruct((depth, CORES, rows, features), jnp.bfloat16))
+        out_specs.append(ANY)
+        scratch += [dma((depth,)) for _ in range(4)] + [dma]
+    return pl.pallas_call(
+        functools.partial(join_kernel, depth, gather),
+        out_shape=tuple(out_shape),
+        in_specs=[VMEM] * 5,
+        out_specs=tuple(out_specs),
+        scratch_shapes=scratch,
+        compiler_params=pltpu.CompilerParams(collective_id=number, has_side_effects=True),
+        name=f"join_{number}",
+    )(part, residual, scale[None], gain[None], shift[None])
+
+
+def dot_last(left, right):
+    return lax.dot_general(left, right, (((1,), (1,)), ((), ())), preferred_element_type=jnp.float32)
+
+
+def dot_first(left, right):
+    return lax.dot_general(left, right, (((0,), (0,)), ((), ())), preferred_element_type=jnp.float32)
+
+
+def column_plan(
+    depth, tokens, gate_weight, up_weight, down_weight, gate_scale, up_scale, down_scale,
+    bgate_weight, cgate_weight, value_weight, bgate_scale, cgate_scale, value_scale, conv_taps,
+    mixout_weight, mixout_scale, first_gain, first_shift, mixer_gain, mixer_shift, last_gain, last_shift,
+):
+    z, c = lax.axis_index("z"), lax.axis_index("c")
+    own = lax.all_to_all(tokens, ("x", "c"), 0, 1, tiled=True)
+    rows, features = own.shape
+
+    def cut(matrix):
+        return matrix.astype(jnp.bfloat16).reshape(depth, -1, matrix.shape[1])
+
+    blocks = jnp.concatenate(
+        [cut(gate_weight.T), cut(up_weight.T), cut(down_weight)]
+        + [cut(m.T) for m in (bgate_weight, cgate_weight, value_weight)]
+        + [cut(mixout_weight)],
+        axis=1,
+    )
+    units = gate_weight.shape[1] // depth
+    channels = bgate_weight.shape[1] // depth
+    pieces = (gate_scale, up_scale, down_scale, bgate_scale, cgate_scale, value_scale, mixout_scale)
+    flat = jnp.concatenate([piece.reshape(-1) for piece in pieces])
+    flat = jnp.pad(flat, (0, -flat.shape[0] % 1024)).reshape(-1, 128)
+    kept, scales, gathered = spread_weights(depth, blocks, flat, own)
+    scales = scales.reshape(scales.shape[:4] + (-1,))
+    mine = lax.dynamic_index_in_dim(lax.dynamic_index_in_dim(scales, c, 0, False), z, 2, False)
+    edges = [0]
+    for piece in pieces:
+        edges.append(edges[-1] + piece.shape[1])
+
+    def unit_scale(k):
+        return mine[:, :, edges[k] : edges[k + 1]].reshape(2, -1)
+
+    def feature_scale(k):
+        return scales[..., edges[k] : edges[k + 1]].transpose(1, 0, 3, 2, 4).reshape(-1)
+
+    gate_cols, up_cols = unit_scale(0), unit_scale(1)
+    bgate_cols, cgate_cols, value_cols = unit_scale(3), unit_scale(4), unit_scale(5)
+    down_cols, mixout_cols = HALF_STEP * feature_scale(2), feature_scale(6)
+    taps = conv_taps.reshape(TAPS, 2, CORES, depth, channels)
+    taps = lax.dynamic_index_in_dim(lax.dynamic_index_in_dim(taps, c, 2, False), z, 2, False)
+
+    def shares(total):
+        return total.astype(jnp.bfloat16).reshape(depth, CORES, rows, features)
+
+    def channel_mix(whole):
+        inputs = whole.reshape(-1, features)
+        total = 0.0
+        for k in range(2):
+            sums = dot_last(kept[k, : 2 * units], inputs)
+            gate_sum = sums[:units] * gate_cols[k][:, None]
+            up_sum = sums[units:] * up_cols[k][:, None]
+            hidden = (jax.nn.silu(gate_sum) * up_sum).astype(jnp.bfloat16)
+            total = total + dot_first(hidden, kept[k, 2 * units : 3 * units])
+        return shares(total)
+
+    def token_mix(whole):
+        inputs = whole.reshape(-1, features)
+        base = 3 * units
+        total = 0.0
+        for k in range(2):
+            sums = dot_last(inputs, kept[k, base : base + 3 * channels])
+            outgate = sums[:, :channels] * bgate_cols[k]
+            ingate = sums[:, channels : 2 * channels] * cgate_cols[k]
+            values = sums[:, 2 * channels :] * value_cols[k]
+            mixed = (ingate * values).reshape(-1, LENGTH, channels)
+            padded = jnp.pad(mixed, ((0, 0), (TAPS - 1, 0), (0, 0)))
+            convolved = jnp.zeros(mixed.shape, jnp.float32)
+            for tap in range(TAPS):
+                convolved = convolved + taps[tap, k] * padded[:, tap : tap + LENGTH]
+            gated = (outgate * convolved.reshape(-1, channels)).astype(jnp.bfloat16)
+            total = total + jnp.dot(
+                gated, kept[k, base + 3 * channels :], preferred_element_type=jnp.float32
+            )
+        return shares(total)
+
+    first, gathered = join(depth, True, 1, channel_mix(gathered), own, down_cols, first_gain, first_shift)
+    second, gathered = join(depth, True, 2, token_mix(gathered), first, mixout_cols, mixer_gain, mixer_shift)
+    (last,) = join(depth, False, 3, channel_mix(gathered), second, down_cols, last_gain, last_shift)
+    return lax.all_to_all(last, ("x", "c"), 1, 0, tiled=True)
 
 
 def add_rows(gathered, shard_piece):
@@ -162,4 +485,20 @@
         P(),
     )
     out_specs = P("fs", "tp")
+    across = mesh.shape["tp"] // CORES
+    if across == 2 and mesh.shape["fs"] % 2 == 0 and mesh.shape["fs"] > 2:
+        depth = mesh.shape["fs"] // 2
+        fine = Mesh(mesh.devices.reshape(depth, 2, 2, CORES), ("z", "y", "x", "c"))
+        names = {"fs": ("z", "y"), "tp": ("x", "c")}
+
+        def split(spec):
+            return P(*(names.get(name) for name in spec))
+
+        return jax.shard_map(
+            functools.partial(column_plan, depth),
+            mesh=fine,
+            in_specs=tuple(split(spec) for spec in in_specs),
+            out_specs=split(out_specs),
+            check_vma=False,
+        )
     return jax.shard_map(shards, mesh=mesh, in_specs=in_specs, out_specs=out_specs, check_vma=False)

time: 670 us -> 392 us (0.59)
  waiting for transfers between devices: 536 us -> 0.01 us
  Pallas kernels: 0 us -> 309 us
  blocking collectives: 56.8 us -> 8.61 us
  between operations: 14.8 us -> 0.37 us
  other arithmetic: 16.5 us -> 5.15 us
  local copies, waits for them, and re-layouts: 7.65 us -> 17.6 us
    all_gather x10 -> x0, waiting for transfers between devices: 469 us -> none  [the longest x1 93.2 us: shards(): kept_down = lax.all_gather(down_low, 'fs', axis=1, tiled=True)]
    pallas_call x0 -> x4, Pallas kernels: none -> 309 us  [the longest x3 156 us: join(): pl.pallas_call(functools.partial(join_kernel, depth, gather), out_shape=t...]
    reduce_scatter x3 -> x0, waiting for transfers between devices: 65.6 us -> none  [spread_back(): lax.psum_scatter(lax.dot_general(weight_cols, left_rows, (((0,), (1,)), (...]
    unnamed x1 -> x0, blocking collectives: 39.5 us -> none
    psum x3 -> x0, blocking collectives: 17.3 us -> none  [post_norm(): lax.psum((jnp.sum(summed, -1), jnp.sum(summed * summed, -1)), 'tp')]
    all_to_all x0 -> x1, blocking collectives: none -> 8.61 us  [column_plan(): return lax.all_to_all(last, ('x', 'c'), 1, 0, tiled=True)]
    convert_element_type x10 -> x9, other arithmetic: 12.7 us -> 4.84 us  [the longest x7 4.77 us: cut(): return matrix.astype(jnp.bfloat16).reshape(depth, -1, matrix.shape[1])]
    dot_general x7 -> x12, matrix products: 37.3 us -> 42.5 us  [the longest x6 22.8 us: dot_last(): lax.dot_general(left, right, (((1,), (1,)), ((), ())), preferred_element_...]
  transfers between devices with their start and end apart: 13 -> 1, of which waited for: 12 -> 0; matrix products, arithmetic and copies ran while one was open for 4% -> 4% of each run, Pallas kernels for 0% -> 0%
where the time goes in v1:
time: 392 us; the launch traced here: 388 us
  Pallas kernels  309 us (79%)
  matrix products  42.5 us (11%)
  local copies, waits for them, and re-layouts  17.6 us (4%)
  blocking collectives  8.61 us (2%)
  other arithmetic  5.15 us (1%)
  starting transfers between devices  4.38 us (1%)
    pallas_call x3, Pallas kernels, join(): pl.pallas_call(functools.partial(join_kernel, depth, gather), out_shape=t...  156 us
    pallas_call x1, Pallas kernels, spread_weights(): pl.pallas_call(functools.partial(weights_kernel, depth), out_shape=(jax.S...  153 us
    dot_general x6, matrix products, dot_last(): lax.dot_general(left, right, (((1,), (1,)), ((), ())), preferred_element_...  22.8 us
    dot_general x4, matrix products, dot_first(): lax.dot_general(left, right, (((0,), (0,)), ((), ())), preferred_element_...  14.7 us
    all_to_all x1, blocking collectives, column_plan(): return lax.all_to_all(last, ('x', 'c'), 1, 0, tiled=True)  8.61 us
  transfers between devices with their start and end apart: 1, of which 0 were waited for; matrix products, arithmetic and copies ran while one was open for 4% of the time, Pallas kernels for 0%

profile of v1, /device:TPU:0, one launch (start us, length us, event | category | flops | bytes accessed | tf_op | source)
XLA Modules:
  0.0 387.7 jit_solution(2592937133263052574)
XLA Ops:
  0.0 4.4 %all-to-all-start = ((bf16[4,64,512]{2,1,0:T(8,128)(2,1)}), bf16[4,64,512]{2,1,0:T(8,128)(2,1)}, u32[]{:S(2)}, u32[]{:S(2)}) async-start(bf16[4,64,512]{2,1,0:T(8,128)(2,1)} %bitcast.134), calls=%async_computation | async-start | bytes 524288 | tf_op jit(solution)/shard_map/all_to_all | solution.py:262
  4.4 0.8 concatenate.7
  5.2 0.6 pad_bitcast_fusion.s_ref
  5.8 0.8 reshape.152
  6.6 1.1 convert_bitcast_fusion.4
  7.7 0.8 copy.34
  8.5 1.1 convert_bitcast_fusion.3
  9.6 0.8 copy.35
  10.5 0.9 copy.36
  11.5 1.2 copy.32
  12.6 1.5 convert_bitcast_fusion
  14.2 1.2 copy.33
  15.4 0.9 convert_element_type.72
  16.3 1.2 constant_dynamic-update-slice_fusion.6
  17.5 1.2 constant_dynamic-update-slice_fusion.5
  18.7 1.2 constant_dynamic-update-slice_fusion.4
  20.1 1.9 copy.45
  22.0 152.7 %spread_weights.1 = (bf16[2,1568,2048]{2,1,0:T(8,128)(2,1)}, f32[2,2,2,4,8,128]{5,4,3,2,1,0:T(8,128)}, bf16[4,2,64,2048]{3,2,1,0:T(8,128)(2,1)}) custom-call(bf16[4,1568,256]{2,1,0:T(8,128)(2,1)} %copy-done, f32[8,128]{1,0:T(8,128)} %pad_bitcast_fusion.s_ref, bf16[64,2048]{1,0:T(8,128)(2,1)} %bitcast.121), custom_call_target="tpu_custom_call" | custom-call | tf_op jit(solution)/shard_map/spread_weights/pallas_call | solution.py:165
  174.7 0.9 reshape.149
  175.9 4.3 %fusion.2 = f32[704,512]{1,0:T(8,128)S(1)} fusion(bf16[512,2048]{1,0:T(8,128)(2,1)} %bitcast.151, bf16[2,1568,2048]{2,1,0:T(8,128)(2,1)} %get-tuple-element.12), kind=kOutput, calls=%fused_computation.5 | convolution fusion | flops 1476395008 | bytes 6422528 | tf_op jit(solution)/shard_map/dot_general | solution.py:249
  180.3 4.6 %fusion.6 = f32[704,512]{1,0:T(8,128)} fusion(bf16[512,2048]{1,0:T(8,128)(2,1)S(1)} %bitcast.152, bf16[2,1568,2048]{2,1,0:T(8,128)(2,1)} %get-tuple-element.12), kind=kOutput, calls=%fused_computation.9 | convolution fusion | flops 1476395008 | bytes 6422528 | tf_op jit(solution)/shard_map/dot_general | solution.py:249
  184.9 0.7 mul.259.scale_ref
  185.6 0.1 mul.248
  185.7 0.1 mul.252
  185.7 0.1 mul.244
  185.8 0.1 mul.240
  185.9 3.3 fusion.22
  189.2 4.3 %add_convert_fusion.2 = bf16[512,2048]{1,0:T(8,128)(2,1)} fusion(f32[512,2048]{1,0:T(8,128)S(1)} %fusion.22, bf16[2,1568,2048]{2,1,0:T(8,128)(2,1)} %get-tuple-element.12, f32[704,512]{1,0:T(8,128)S(1)} %fusion.2, f32[352]{0:T(512)S(1)} %mul.252, f32[352]{0:T(512)S(1)} %mul.248), kind=kOutput, calls=%fused_computation.2 | convolution fusion | flops 741736448 | bytes 9177856 | tf_op jit(solution)/shard_map/dot_general | solution.py:253
  193.5 66.8 %join_1.1 = (bf16[64,2048]{1,0:T(8,128)(2,1)}, bf16[4,2,64,2048]{3,2,1,0:T(8,128)(2,1)}) custom-call(bf16[4,2,64,2048]{3,2,1,0:T(8,128)(2,1)} %bitcast.124, bf16[64,2048]{1,0:T(8,128)(2,1)} %bitcast.122, f32[1,2048]{1,0:T(1,128)} %mul.259.scale_ref, f32[1,2048]{1,0:T(1,128)} %bitcast.138, f32[1,2048]{1,0:T(1,128)} %bitcast.139), custom_call_target="tpu_custom_call" | custom-call | tf_op jit(solution)/shard_map/join_1/pallas_call | solution.py:237
  260.3 3.5 fusion.12
  263.8 2.7 fusion.14
  266.5 0.1 mul.280
  266.5 0.1 mul.288
  266.6 0.1 mul.285
  267.0 0.7 broadcast_in_dim_reshape.3.scale_ref
  267.7 0.1 fusion.59
  267.8 1.7 fusion.37
  269.6 0.1 fusion.63
  269.7 3.2 add_convert_fusion.1
  273.0 56.9 %join_2.1 = (bf16[64,2048]{1,0:T(8,128)(2,1)}, bf16[4,2,64,2048]{3,2,1,0:T(8,128)(2,1)}) custom-call(bf16[4,2,64,2048]{3,2,1,0:T(8,128)(2,1)} %bitcast.117, bf16[64,2048]{1,0:T(8,128)(2,1)} %get-tuple-element.16.res_ref, f32[1,2048]{1,0:T(1,128)} %broadcast_in_dim_reshape.3.scale_ref, f32[1,2048]{1,0:T(1,128)} %bitcast.140, f32[1,2048]{1,0:T(1,128)} %bitcast.141), custom_call_target="tpu_custom_call" | custom-call | tf_op jit(solution)/shard_map/join_2/pallas_call | solution.py:237
  329.9 4.3 %fusion = f32[704,512]{1,0:T(8,128)S(1)} fusion(bf16[512,2048]{1,0:T(8,128)(2,1)} %bitcast.153, bf16[2,1568,2048]{2,1,0:T(8,128)(2,1)} %get-tuple-element.12), kind=kOutput, calls=%fused_computation.3 | convolution fusion | flops 1476395008 | bytes 6422528 | tf_op jit(solution)/shard_map/dot_general | solution.py:249
  334.2 3.5 fusion.4
  337.7 2.9 fusion.20
  340.6 4.3 %add_convert_fusion = bf16[512,2048]{1,0:T(8,128)(2,1)} fusion(f32[512,2048]{1,0:T(8,128)S(1)} %fusion.20, bf16[2,1568,2048]{2,1,0:T(8,128)(2,1)} %get-tuple-element.12, f32[704,512]{1,0:T(8,128)S(1)} %fusion, f32[352]{0:T(512)S(1)} %mul.252, f32[352]{0:T(512)S(1)} %mul.248), kind=kOutput, calls=%fused_computation | convolution fusion | flops 741736448 | bytes 9177856 | tf_op jit(solution)/shard_map/dot_general | solution.py:253
  344.9 32.5 %join_3.1 = bf16[64,2048]{1,0:T(8,128)(2,1)} custom-call(bf16[4,2,64,2048]{3,2,1,0:T(8,128)(2,1)} %bitcast.123, bf16[64,2048]{1,0:T(8,128)(2,1)} %get-tuple-element.18.res_ref, f32[1,2048]{1,0:T(1,128)} %mul.259.scale_ref, f32[1,2048]{1,0:T(1,128)} %bitcast.142, f32[1,2048]{1,0:T(1,128)} %bitcast.143), custom_call_target="tpu_custom_call" | custom-call | tf_op jit(solution)/shard_map/join_3/pallas_call | solution.py:237
  377.4 1.0 copy.51
  378.3 8.6 %all_to_all.38 = bf16[64,4,512]{2,0,1:T(8,128)(2,1)S(1)} all-to-all(bf16[64,4,512]{2,0,1:T(8,128)(2,1)S(1)} %bitcast.132), channel_id=1, replica_groups=mesh['z'=4,'y'=2,'x'=2,'c'=2] {'x','c'}, dimensions={1} | all-to-all | bytes 524288 | tf_op jit(solution)/shard_map/all_to_all | solution.py:335
  386.9 0.7 copy.60
  (45 shorter events, 0.9 us)
Async XLA Ops:
  0.0 10.4 %copy-start.6 = (f32[256,512]{1,0:T(8,128)S(1)}, f32[256,512]{1,0:T(8,128)}, u32[]{:S(2)}) copy-start(f32[256,512]{1,0:T(8,128)} %param.31) | copy-start | bytes 1572868
  0.0 11.3 %copy-start.7 = (f32[512,256]{1,0:T(8,128)S(1)}, f32[512,256]{1,0:T(8,128)}, u32[]{:S(2)}) copy-start(f32[512,256]{1,0:T(8,128)} %param.36) | copy-start | bytes 1572868
  0.0 11.4 %copy-start.1 = (f32[256,1408]{1,0:T(8,128)S(1)}, f32[256,1408]{1,0:T(8,128)}, u32[]{:S(2)}) copy-start(f32[256,1408]{1,0:T(8,128)} %param.23) | copy-start | bytes 4325380
  0.0 20.1 %all-to-all-start = ((bf16[4,64,512]{2,1,0:T(8,128)(2,1)}), bf16[4,64,512]{2,1,0:T(8,128)(2,1)}, u32[]{:S(2)}, u32[]{:S(2)}) async-start(bf16[4,64,512]{2,1,0:T(8,128)(2,1)} %bitcast.134), calls=%async_computation | async-start | bytes 524288 | tf_op jit(solution)/shard_map/all_to_all | solution.py:262
  12.6 2.7 copy-start.2
  17.5 2.4 copy-start.3
  17.5 2.5 copy-start.4
  17.5 2.5 copy-start.5
  20.0 1.9 copy-start
  175.9 4.3 %copy-start.8 = (bf16[4,2,64,2048]{3,2,1,0:T(8,128)(2,1)S(1)}, bf16[4,2,64,2048]{3,2,1,0:T(8,128)(2,1)}, u32[]{:S(2)}) copy-start(bf16[4,2,64,2048]{3,2,1,0:T(8,128)(2,1)} %get-tuple-element.13) | copy-start | bytes 6291460
  260.3 3.5 copy-start.10
  329.9 4.3 %copy-start.9 = (bf16[4,2,64,2048]{3,2,1,0:T(8,128)(2,1)S(1)}, bf16[4,2,64,2048]{3,2,1,0:T(8,128)(2,1)}, u32[]{:S(2)}) copy-start(bf16[4,2,64,2048]{3,2,1,0:T(8,128)(2,1)} %get-tuple-element.17) | copy-start | bytes 6291460

commit v2 on v0

--- a/solution.py
+++ b/solution.py
@@ -1,15 +1,398 @@
+import functools
+
 import jax
 import jax.numpy as jnp
 from jax import lax
+from jax.experimental import pallas as pl
+from jax.experimental.pallas import tpu as pltpu
+from jax.sharding import Mesh
 from jax.sharding import PartitionSpec as P
 
 TAPS = 3
 LENGTH = 128
-
+CORES = 2
 
 RESIDUAL_SCALE = 1.4142135623730951
 HALF_STEP = 0.5
 EPSILON = 1e-05
+BY_AXIS = pl.DeviceIdType.MESH
+ANY = pl.BlockSpec(memory_space=pl.ANY)
+VMEM = pl.BlockSpec(memory_space=pltpu.VMEM)
+
+
+def greet(depth, axes):
+    barrier = pltpu.get_barrier_semaphore()
+    z = lax.axis_index("z")
+    targets = [{"z": lax.rem(z + d, depth)} for d in range(1, depth)]
+    targets += [{axis: 1 - lax.axis_index(axis)} for axis in axes]
+    for target in targets:
+        pl.semaphore_signal(barrier, inc=1, device_id=target, device_id_type=BY_AXIS)
+    pl.semaphore_wait(barrier, len(targets))
+
+
+def remote(src, dst, send, recv, target):
+    return pltpu.make_async_remote_copy(
+        src_ref=src, dst_ref=dst, send_sem=send, recv_sem=recv, device_id=target, device_id_type=BY_AXIS
+    )
+
+
+def block_place(ref, px, pz, py, width):
+    start = pl.multiple_of((pz * 2 + py) * width, width)
+    return ref.at[:, px, :, pl.ds(start, width)]
+
+
+def weights_kernel(
+    depth, w_ref, m_ref, s_ref, t_ref, g_ref, held_ref, sa_ref, ta_ref,
+    zsend, zrecv, ysend, yrecv, xsend, xrecv, dsend, drecv, msend, mrecv,
+    ssend, srecv, tzsend, tzrecv, tcsend, tcrecv, local,
+):
+    z, y, x, c = (lax.axis_index(axis) for axis in ("z", "y", "x", "c"))
+    width = w_ref.shape[-1]
+    greet(depth, ("y", "x", "c"))
+
+    def place(px, pz, py):
+        return block_place(g_ref, px, pz, py, width)
+
+    to_x, to_y, to_c = {"x": 1 - x}, {"y": 1 - y}, {"c": 1 - c}
+    scale_sends, token_sends, z_copies, m_copies = [], [], [], []
+    keeps = [
+        pltpu.make_async_copy(s_ref, sa_ref.at[c, x, y, z], local.at[0]),
+        pltpu.make_async_copy(t_ref, ta_ref.at[0, c], local.at[1]),
+        pltpu.make_async_copy(w_ref.at[z], place(x, z, y), local.at[2]),
+        pltpu.make_async_copy(m_ref.at[z], held_ref.at[0], local.at[3]),
+    ]
+    for copy in keeps:
+        copy.start()
+    beside = [remote(t_ref, ta_ref.at[0, c], tcsend.at[0], tcrecv.at[0], to_c)]
+    beside[0].start()
+    own_y = remote(w_ref.at[z], place(x, z, y), ysend.at[0], yrecv.at[0], to_y)
+    own_x = remote(w_ref.at[z], place(x, z, y), xsend.at[0], xrecv.at[0], to_x)
+    own_y.start()
+    own_x.start()
+    y_copies, x_copies, d_copies = [own_y], [own_x], []
+    for d in range(1, depth):
+        target = {"z": lax.rem(z + d, depth)}
+        scale_sends.append(remote(s_ref, sa_ref.at[c, x, y, z], ssend.at[d], srecv.at[d], target))
+        scale_sends[-1].start()
+    for d in range(1, depth):
+        target = lax.rem(z + d, depth)
+        z_copies.append(remote(w_ref.at[target], place(x, z, y), zsend.at[d], zrecv.at[d], {"z": target}))
+        z_copies[-1].start()
+    for d in range(1, depth):
+        target = {"z": lax.rem(z + d, depth)}
+        token_sends.append(remote(t_ref, ta_ref.at[d, c], tzsend.at[d], tzrecv.at[d], target))
+        token_sends[-1].start()
+    for d in range(1, depth):
+        target = lax.rem(z + d, depth)
+        m_copies.append(remote(m_ref.at[target], held_ref.at[d], msend.at[d], mrecv.at[d], {"z": target}))
+        m_copies[-1].start()
+
+    def relay(d):
+        source = lax.rem(z - d + depth, depth)
+        if d % 2 == 0:
+            y_copies[d].wait_recv()
+            block = place(x, source, 1 - y)
+            copy = remote(block, block, dsend.at[d], drecv.at[d], to_x)
+        else:
+            x_copies[d].wait_recv()
+            block = place(1 - x, source, y)
+            copy = remote(block, block, dsend.at[d], drecv.at[d], to_y)
+        copy.start()
+        d_copies.append(copy)
+
+    keeps[0].wait()
+    for copy in scale_sends:
+        copy.wait()
+    hops = (sa_ref.at[c, x, y], sa_ref.at[c, x], sa_ref.at[c])
+    for k, (part, target) in enumerate(zip(hops, (to_y, to_x, to_c))):
+        slot = (0, depth, depth + 1)[k]
+        hop = remote(part, part, ssend.at[slot], srecv.at[slot], target)
+        hop.start()
+        hop.wait()
+    for d in range(1, depth):
+        block = place(x, lax.rem(z - d + depth, depth), y)
+        z_copies[d - 1].wait_recv()
+        ycopy = remote(block, block, ysend.at[d], yrecv.at[d], to_y)
+        xcopy = remote(block, block, xsend.at[d], xrecv.at[d], to_x)
+        ycopy.start()
+        xcopy.start()
+        y_copies.append(ycopy)
+        x_copies.append(xcopy)
+        relay(d - 1)
+    relay(depth - 1)
+    for d in range(1, depth):
+        token_sends[d - 1].wait_recv()
+        copy = remote(ta_ref.at[d, c], ta_ref.at[d, c], tcsend.at[d], tcrecv.at[d], to_c)
+        copy.start()
+        beside.append(copy)
+    for d in range(depth):
+        if d % 2 == 0:
+            x_copies[d].wait_recv()
+        else:
+            y_copies[d].wait_recv()
+        d_copies[d].wait_recv()
+        y_copies[d].wait_send()
+        x_copies[d].wait_send()
+        d_copies[d].wait_send()
+        beside[d].wait()
+    for copy in m_copies:
+        copy.wait()
+    for copy in z_copies + token_sends:
+        copy.wait_send()
+    for copy in keeps[1:]:
+        copy.wait()
+
+
+def spread_weights(depth, blocks, mixer_blocks, scale_block, own_rows):
+    mats, rows, width = blocks.shape[1:]
+    dma = pltpu.SemaphoreType.DMA
+    return pl.pallas_call(
+        functools.partial(weights_kernel, depth),
+        out_shape=(
+            jax.ShapeDtypeStruct((mats, 2, rows, depth * 2 * width), jnp.bfloat16),
+            jax.ShapeDtypeStruct(mixer_blocks.shape, jnp.bfloat16),
+            jax.ShapeDtypeStruct((CORES, 2, 2, depth) + scale_block.shape, jnp.float32),
+            jax.ShapeDtypeStruct((depth, CORES) + own_rows.shape, jnp.bfloat16),
+        ),
+        in_specs=[ANY] * 4,
+        out_specs=(ANY,) * 4,
+        scratch_shapes=[dma((depth,)) for _ in range(10)]
+        + [dma((depth + 2,)), dma((depth + 2,))]
+        + [dma((depth,)) for _ in range(4)]
+        + [dma((4,))],
+        compiler_params=pltpu.CompilerParams(collective_id=0, has_side_effects=True),
+        name="spread_weights",
+    )(blocks, mixer_blocks, scale_block, own_rows)
+
+
+def dot_last(left, right):
+    return lax.dot_general(left, right, (((1,), (1,)), ((), ())), preferred_element_type=jnp.float32)
+
+
+def merged(ref, k):
+    two, rows, features = ref.shape[1:]
+    return ref[k].reshape(two * rows, features)
+
+
+def feed_chunk(inputs, weights, factors, taps):
+    gate_sum = dot_last(inputs, merged(weights, 0)) * factors[0:1]
+    up_sum = dot_last(inputs, merged(weights, 1)) * factors[1:2]
+    hidden = (gate_sum / (1.0 + jnp.exp(-gate_sum)) * up_sum).astype(jnp.bfloat16)
+    return jnp.dot(hidden, merged(weights, 2), preferred_element_type=jnp.float32)
+
+
+def mixer_chunk(inputs, weights, factors, taps):
+    outgate = dot_last(inputs, merged(weights, 0)) * factors[0:1]
+    ingate = dot_last(inputs, merged(weights, 1)) * factors[1:2]
+    values = dot_last(inputs, merged(weights, 2)) * factors[2:3]
+    mixed = ingate * values
+    position = lax.rem(lax.broadcasted_iota(jnp.int32, mixed.shape, 0), LENGTH)
+    convolved = taps[TAPS - 1 : TAPS] * mixed
+    for back in range(1, TAPS):
+        earlier = jnp.where(position >= back, pltpu.roll(mixed, back, 0), 0.0)
+        convolved = convolved + taps[TAPS - 1 - back : TAPS - back] * earlier
+    gated = (outgate * convolved).astype(jnp.bfloat16)
+    return jnp.dot(gated, merged(weights, 3), preferred_element_type=jnp.float32)
+
+
+def stage_kernel(depth, chunk, first, *refs):
+    refs = list(refs)
+    take = lambda n: [refs.pop(0) for _ in range(n)]
+    w_ref, f_ref, k_ref, own_ref, scale_ref, gain_ref, shift_ref = take(7)
+    if first:
+        whole, held_ref = take(2)
+        out_ref, m_ref = take(2)
+    else:
+        (out_ref,) = take(1)
+    part, half, sums, got, hsend, hrecv, rsend, rrecv = take(8)
+    z, c = lax.axis_index("z"), lax.axis_index("c")
+    to_c = {"c": 1 - c}
+    if first:
+        ysend, yrecv, xsend, xrecv, dsend, drecv, local = take(7)
+        y, x = lax.axis_index("y"), lax.axis_index("x")
+        greet(depth, ("y", "x", "c"))
+        width = held_ref.shape[-1]
+        y_copies, x_copies, d_copies, keeps = [], [], [], []
+        for d in range(depth):
+            block = block_place(m_ref, x, lax.rem(z - d + depth, depth), y, width)
+            y_copies.append(remote(held_ref.at[d], block, ysend.at[d], yrecv.at[d], {"y": 1 - y}))
+            x_copies.append(remote(held_ref.at[d], block, xsend.at[d], xrecv.at[d], {"x": 1 - x}))
+            keeps.append(pltpu.make_async_copy(held_ref.at[d], block, local.at[d]))
+            y_copies[d].start()
+            x_copies[d].start()
+            keeps[d].start()
+    else:
+        whole, zsend, zrecv, csend, crecv = take(5)
+        greet(depth, ("c",))
+        beside = remote(own_ref, whole.at[0, c], csend.at[0], crecv.at[0], to_c)
+        beside.start()
+        across = []
+        for d in range(1, depth):
+            target = {"z": lax.rem(z + d, depth)}
+            across.append(remote(own_ref, whole.at[d, c], zsend.at[d], zrecv.at[d], target))
+            across[-1].start()
+        whole[0, c] = own_ref[...]
+
+    def share(d):
+        target = {"z": lax.rem(z - d + depth, depth)}
+        return remote(sums.at[d], got.at[d], rsend.at[d], rrecv.at[d], target)
+
+    def handover(d):
+        return remote(part.at[d, 1 - c], half.at[d], hsend.at[d], hrecv.at[d], to_c)
+
+    def forward(d):
+        return remote(whole.at[d, c], whole.at[d, c], csend.at[d], crecv.at[d], to_c)
+
+    def step(i, carry):
+        d = lax.rem(i + 1, depth) if first else i
+        if not first:
+
+            @pl.when(d > 0)
+            def _():
+                remote(own_ref, whole.at[d, c], zsend.at[d], zrecv.at[d], {"z": z}).wait_recv()
+                forward(d).start()
+
+            forward(d).wait_recv()
+        rows = own_ref.shape[0]
+        inputs = whole[d].reshape(CORES * rows, -1)
+        total = chunk(inputs, w_ref, f_ref[...], k_ref[...])
+        part[d] = total.astype(jnp.bfloat16).reshape(part.shape[1:])
+        handover(d).start()
+        handover(d).wait_recv()
+
+        @pl.when(d > 0)
+        def _():
+            both = part[d, c].astype(jnp.float32) + half[d].astype(jnp.float32)
+            sums[d] = both.astype(jnp.bfloat16)
+            share(d).start()
+
+        return carry
+
+    lax.fori_loop(0, depth, step, 0)
+    if first:
+        for d in range(depth):
+            source = lax.rem(z - d + depth, depth)
+            if d % 2 == 0:
+                y_copies[d].wait_recv()
+                block = block_place(m_ref, x, source, 1 - y, width)
+                copy = remote(block, block, dsend.at[d], drecv.at[d], {"x": 1 - x})
+            else:
+                x_copies[d].wait_recv()
+                block = block_place(m_ref, 1 - x, source, y, width)
+                copy = remote(block, block, dsend.at[d], drecv.at[d], {"y": 1 - y})
+            copy.start()
+            d_copies.append(copy)
+    total = part[0, c].astype(jnp.float32) + half[0].astype(jnp.float32)
+    for d in range(1, depth):
+        share(d).wait_recv()
+        total = total + got[d].astype(jnp.float32)
+    summed = RESIDUAL_SCALE * own_ref[...].astype(jnp.float32) + total * scale_ref[...]
+    count = summed.shape[1]
+    average = jnp.sum(summed, -1, keepdims=True) / count
+    mean_square = jnp.sum(summed * summed, -1, keepdims=True) / count
+    variance = mean_square - average * average
+    normed = (summed - average) * lax.rsqrt(variance + EPSILON) * gain_ref[...] + shift_ref[...]
+    out_ref[...] = normed.astype(jnp.bfloat16)
+    for d in range(depth):
+        handover(d).wait_send()
+        if d > 0:
+            share(d).wait_send()
+    if first:
+        for d in range(depth):
+            (x_copies if d % 2 == 0 else y_copies)[d].wait_recv()
+            for copy in (y_copies[d], x_copies[d]):
+                copy.wait_send()
+            d_copies[d].wait()
+            keeps[d].wait()
+    else:
+        beside.wait_send()
+        for d in range(1, depth):
+            forward(d).wait_send()
+            across[d - 1].wait_send()
+
+
+def stage(depth, number, chunk, weights, factors, taps, own, scale, gain, shift, whole=None, held=None):
+    rows, features = own.shape
+    first = whole is not None
+    dma = pltpu.SemaphoreType.DMA
+    block = pltpu.VMEM((depth, rows, features), jnp.bfloat16)
+    pair = pltpu.VMEM((depth, CORES, rows, features), jnp.bfloat16)
+    operands = [weights, factors, taps, own, scale[None], gain[None], shift[None]]
+    in_specs = [VMEM] * 7
+    out_shape = [jax.ShapeDtypeStruct((rows, features), jnp.bfloat16)]
+    out_specs = [VMEM]
+    scratch = [pair, block, block, block] + [dma((depth,)) for _ in range(4)]
+    if first:
+        operands += [whole, held]
+        in_specs += [VMEM, ANY]
+        mats, part_rows, width = held.shape[1:]
+        out_shape.append(jax.ShapeDtypeStruct((mats, 2, part_rows, depth * 2 * width), jnp.bfloat16))
+        out_specs.append(ANY)
+        scratch += [dma((depth,)) for _ in range(7)]
+    else:
+        scratch += [pair] + [dma((depth,)) for _ in range(4)]
+    return pl.pallas_call(
+        functools.partial(stage_kernel, depth, chunk, first),
+        out_shape=tuple(out_shape),
+        in_specs=in_specs,
+        out_specs=tuple(out_specs),
+        scratch_shapes=scratch,
+        compiler_params=pltpu.CompilerParams(
+            collective_id=number, has_side_effects=True, vmem_limit_bytes=40 * 1024 * 1024
+        ),
+        name=f"stage_{number}",
+    )(*operands)
+
+
+def column_plan(
+    depth, tokens, gate_weight, up_weight, down_weight, gate_scale, up_scale, down_scale,
+    bgate_weight, cgate_weight, value_weight, bgate_scale, cgate_scale, value_scale, conv_taps,
+    mixout_weight, mixout_scale, first_gain, first_shift, mixer_gain, mixer_shift, last_gain, last_shift,
+):
+    z, c = lax.axis_index("z"), lax.axis_index("c")
+    own = lax.all_to_all(tokens, ("x", "c"), 0, 1, tiled=True)
+
+    def cut(matrix):
+        return matrix.astype(jnp.bfloat16).reshape(depth, -1, matrix.shape[1])
+
+    blocks = jnp.stack([cut(gate_weight.T), cut(up_weight.T), cut(down_weight)], axis=1)
+    mixer_blocks = jnp.stack(
+        [cut(m.T) for m in (bgate_weight, cgate_weight, value_weight)] + [cut(mixout_weight)], axis=1
+    )
+    channels = bgate_weight.shape[1] // depth
+    pieces = (gate_scale, up_scale, down_scale, bgate_scale, cgate_scale, value_scale, mixout_scale)
+    flat = jnp.concatenate([piece.reshape(-1) for piece in pieces])
+    flat = jnp.pad(flat, (0, -flat.shape[0] % 1024)).reshape(-1, 128)
+    feed_weights, held, scales, whole = spread_weights(depth, blocks, mixer_blocks, flat, own)
+    scales = scales.reshape(scales.shape[:4] + (-1,))
+    mine = lax.dynamic_index_in_dim(lax.dynamic_index_in_dim(scales, c, 0, False), z, 2, False)
+    edges = [0]
+    for piece in pieces:
+        edges.append(edges[-1] + piece.shape[1])
+
+    def unit_scale(k):
+        return mine[:, :, edges[k] : edges[k + 1]].reshape(-1)
+
+    def feature_scale(k):
+        return scales[..., edges[k] : edges[k + 1]].transpose(1, 0, 3, 2, 4).reshape(-1)
+
+    feed_factors = jnp.stack([unit_scale(0), unit_scale(1)])
+    mixer_factors = jnp.stack([unit_scale(3), unit_scale(4), unit_scale(5)])
+    down_cols, mixout_cols = HALF_STEP * feature_scale(2), feature_scale(6)
+    taps = conv_taps.reshape(TAPS, 2, CORES, depth, channels)
+    taps = lax.dynamic_index_in_dim(lax.dynamic_index_in_dim(taps, c, 2, False), z, 2, False)
+    taps = taps.reshape(TAPS, -1)
+
+    first, mixer_weights = stage(
+        depth, 1, feed_chunk, feed_weights, feed_factors, taps, own, down_cols, first_gain, first_shift, whole, held
+    )
+    (second,) = stage(
+        depth, 2, mixer_chunk, mixer_weights, mixer_factors, taps, first, mixout_cols, mixer_gain, mixer_shift
+    )
+    (last,) = stage(
+        depth, 3, feed_chunk, feed_weights, feed_factors, taps, second, down_cols, last_gain, last_shift
+    )
+    return lax.all_to_all(last, ("x", "c"), 1, 0, tiled=True)
 
 
 def add_rows(gathered, shard_piece):
@@ -162,4 +545,20 @@
         P(),
     )
     out_specs = P("fs", "tp")
+    across = mesh.shape["tp"] // CORES
+    if across == 2 and mesh.shape["fs"] % 2 == 0 and mesh.shape["fs"] > 2:
+        depth = mesh.shape["fs"] // 2
+        fine = Mesh(mesh.devices.reshape(depth, 2, 2, CORES), ("z", "y", "x", "c"))
+        names = {"fs": ("z", "y"), "tp": ("x", "c")}
+
+        def split(spec):
+            return P(*(names.get(name) for name in spec))
+
+        return jax.shard_map(
+            functools.partial(column_plan, depth),
+            mesh=fine,
+            in_specs=tuple(split(spec) for spec in in_specs),
+            out_specs=split(out_specs),
+            check_vma=False,
+        )
     return jax.shard_map(shards, mesh=mesh, in_specs=in_specs, out_specs=out_specs, check_vma=False)

time: 670 us -> 304 us (0.45)
  waiting for transfers between devices: 536 us -> 0.01 us
  Pallas kernels: 0 us -> 271 us
  blocking collectives: 56.8 us -> 8.39 us
  matrix products: 37.3 us -> 0 us
  between operations: 14.8 us -> 0.33 us
  other arithmetic: 16.5 us -> 8 us
    all_gather x10 -> x0, waiting for transfers between devices: 469 us -> none  [the longest x1 93.2 us: shards(): kept_down = lax.all_gather(down_low, 'fs', axis=1, tiled=True)]
    pallas_call x0 -> x4, Pallas kernels: none -> 271 us  [the longest x3 173 us: stage(): pl.pallas_call(functools.partial(stage_kernel, depth, chunk, first), out_...]
    reduce_scatter x3 -> x0, waiting for transfers between devices: 65.6 us -> none  [spread_back(): lax.psum_scatter(lax.dot_general(weight_cols, left_rows, (((0,), (1,)), (...]
    unnamed x1 -> x0, blocking collectives: 39.5 us -> none
    dot_general x7 -> x0, matrix products: 37.3 us -> none  [the longest x3 22.6 us: spread_back(): lax.dot_general(weight_cols, left_rows, (((0,), (1,)), ((), ())), preferr...]
    psum x3 -> x0, blocking collectives: 17.3 us -> none  [post_norm(): lax.psum((jnp.sum(summed, -1), jnp.sum(summed * summed, -1)), 'tp')]
    all_to_all x0 -> x1, blocking collectives: none -> 8.39 us  [column_plan(): return lax.all_to_all(last, ('x', 'c'), 1, 0, tiled=True)]
    convert_element_type x10 -> x7, other arithmetic: 12.7 us -> 5.23 us  [cut(): return matrix.astype(jnp.bfloat16).reshape(depth, -1, matrix.shape[1])]
  transfers between devices with their start and end apart: 13 -> 1, of which waited for: 12 -> 0; matrix products, arithmetic and copies ran while one was open for 4% -> 4% of each run, Pallas kernels for 0% -> 0%
where the time goes in v2:
time: 304 us
  Pallas kernels  271 us (89%)
  local copies, waits for them, and re-layouts  11.4 us (4%)
  blocking collectives  8.39 us (3%)
  other arithmetic  8 us (3%)
  starting transfers between devices  4.37 us (1%)
    pallas_call x3, Pallas kernels, stage(): pl.pallas_call(functools.partial(stage_kernel, depth, chunk, first), out_...  173 us
    pallas_call x1, Pallas kernels, spread_weights(): pl.pallas_call(functools.partial(weights_kernel, depth), out_shape=(jax.S...  98.4 us
    all_to_all x1, blocking collectives, column_plan(): return lax.all_to_all(last, ('x', 'c'), 1, 0, tiled=True)  8.39 us
  transfers between devices with their start and end apart: 1, of which 0 were waited for; matrix products, arithmetic and copies ran while one was open for 4% of the time, Pallas kernels for 0%

profile of v2, /device:TPU:0, one launch (start us, length us, event | category | flops | bytes accessed | tf_op | source)
XLA Modules:
  0.0 303.6 jit_solution(4527229140354463699)
XLA Ops:
  0.0 4.4 %all-to-all-start = ((bf16[4,64,512]{2,1,0:T(8,128)(2,1)}), bf16[4,64,512]{2,1,0:T(8,128)(2,1)S(1)}, u32[]{:S(2)}, u32[]{:S(2)}) async-start(bf16[4,64,512]{2,1,0:T(8,128)(2,1)} %bitcast.83), calls=%async_computation | async-start | bytes 524288 | tf_op jit(solution)/shard_map/all_to_all | solution.py:353
  4.4 0.8 concatenate.3
  5.2 0.6 pad_bitcast_fusion.s_ref
  5.8 0.8 reshape.66
  6.6 1.1 convert_bitcast_fusion.4
  7.7 0.0 copy-start.9
  7.7 0.8 copy.35
  8.6 0.9 copy.36
  9.4 0.8 copy.37
  10.3 1.1 convert_element_type.49
  11.4 0.1 convert_bitcast_fusion.1
  11.5 0.0 copy-start.10
  11.5 0.0 copy-start.11
  11.5 0.0 copy-start.12
  11.5 1.5 convert_bitcast_fusion
  13.0 1.1 pad_maximum_fusion.1.m_ref
  14.2 0.3 copy.33
  14.4 0.3 copy.34
  14.7 1.4 convert_element_type.42
  16.2 1.6 pad_maximum_fusion.w_ref
  17.7 0.0 all-to-all-done
  17.7 0.7 copy.48
  18.5 98.4 %spread_weights.1 = (bf16[3,2,352,2048]{3,2,1,0:T(8,128)(2,1)}, bf16[4,4,128,256]{3,2,1,0:T(8,128)(2,1)}, f32[2,2,2,4,8,128]{5,4,3,2,1,0:T(8,128)}, bf16[4,2,64,2048]{3,2,1,0:T(8,128)(2,1)}) custom-call(bf16[4,3,352,256]{3,2,1,0:T(8,128)(2,1)} %pad_maximum_fusion.w_ref, bf16[4,4,128,256]{3,2,1,0:T(8,128)(2,1)} %pad_maximum_fusion.1.m_ref, ...), custom_call_target="tpu_custom_call" | custom-call | tf_op jit(solution)/shard_map/spread_weights/pallas_call | solution.py:149
  116.9 0.9 reshape.65
  117.8 0.1 fusion
  117.9 0.1 fusion.1
  118.0 0.1 fusion.2
  118.1 0.1 mul.22.refs_4_
  118.2 0.1 stack_reshape.43
  118.3 0.1 stack_reshape.45
  118.4 0.1 stack_reshape.47
  118.5 0.1 stack_reshape.46
  118.5 0.1 stack_reshape.44
  118.6 0.1 broadcast_in_dim_reshape.3.refs_4_
  118.8 1.6 copy-done.1
  120.4 1.2 copy-done.2
  121.6 54.3 %stage_1.1 = (bf16[64,2048]{1,0:T(8,128)(2,1)S(1)}, bf16[4,2,128,2048]{3,2,1,0:T(8,128)(2,1)S(1)}) custom-call(bf16[3,2,352,2048]{3,2,1,0:T(8,128)(2,1)} %get-tuple-element.11.refs_0_, f32[2,704]{1,0:T(2,128)S(1)} %pad_maximum_fusion.2.refs_1_, f32[3,256]{1,0:T(4,128)S(1)} %bitcast.64, bf16[64,2048]{1,0:T(8,128)(2,1)S(1)} %bitcast.62, ...), custom_call_target="tpu_custom_call" | custom-call | tf_op jit(solution)/shard_map/stage_1/pallas_call | solution.py:334
  175.9 0.0 copy-start.7
  175.9 0.0 copy-start.8
  176.0 62.1 %stage_2.1.refs_3_ = bf16[64,2048]{1,0:T(8,128)(2,1)S(1)} custom-call(bf16[4,2,128,2048]{3,2,1,0:T(8,128)(2,1)S(1)} %get-tuple-element.15.refs_0_, f32[3,256]{1,0:T(4,128)S(1)} %pad_maximum_fusion.3.refs_1_, f32[3,256]{1,0:T(4,128)S(1)} %bitcast.65, bf16[64,2048]{1,0:T(8,128)(2,1)S(1)} %get-tuple-element.16.refs_3_, ...), custom_call_target="tpu_custom_call" | custom-call | tf_op jit(solution)/shard_map/stage_2/pallas_call | solution.py:334
  238.1 0.0 slice-done
  238.1 0.0 slice-done.1
  238.1 0.0 slice-done.2
  238.1 0.0 copy-done.7
  238.1 0.0 copy-done.8
  238.1 56.3 %stage_3.1 = bf16[64,2048]{1,0:T(8,128)(2,1)S(1)} custom-call(bf16[3,2,352,2048]{3,2,1,0:T(8,128)(2,1)S(1)} %bitcast.60, f32[2,704]{1,0:T(2,128)S(1)} %pad_maximum_fusion.2.refs_1_, f32[3,256]{1,0:T(4,128)S(1)} %bitcast.66, bf16[64,2048]{1,0:T(8,128)(2,1)S(1)} %stage_2.1.refs_3_, f32[1,2048]{1,0:T(1,128)S(1)} %mul.22.refs_4_, f32[1,2048]{1,0:T(1,128)S(1)} %bitcast.71, ...), custom_call_target="tpu_custom_call" | custom-call | tf_op jit(solution)/shard_map/stage_3/pallas_call | solution.py:334
  294.5 8.4 %all_to_all.38 = bf16[64,4,512]{2,0,1:T(8,128)(2,1)S(1)} all-to-all(bf16[64,4,512]{2,0,1:T(8,128)(2,1)S(1)} %bitcast.77), channel_id=1, replica_groups=mesh['z'=4,'y'=2,'x'=2,'c'=2] {'x','c'}, dimensions={1} | all-to-all | bytes 524288 | tf_op jit(solution)/shard_map/all_to_all | solution.py:395
  302.9 0.7 copy.60
  (34 shorter events, 0.2 us)
Async XLA Ops:
  0.0 8.5 %copy-start.13 = (f32[256,512]{1,0:T(8,128)S(1)}, f32[256,512]{1,0:T(8,128)}, u32[]{:S(2)}) copy-start(f32[256,512]{1,0:T(8,128)} %param.30) | copy-start | bytes 1572868
  0.0 9.4 %copy-start.14 = (f32[256,512]{1,0:T(8,128)S(1)}, f32[256,512]{1,0:T(8,128)}, u32[]{:S(2)}) copy-start(f32[256,512]{1,0:T(8,128)} %param.31) | copy-start | bytes 1572868
  0.0 17.7 %all-to-all-start = ((bf16[4,64,512]{2,1,0:T(8,128)(2,1)}), bf16[4,64,512]{2,1,0:T(8,128)(2,1)S(1)}, u32[]{:S(2)}, u32[]{:S(2)}) async-start(bf16[4,64,512]{2,1,0:T(8,128)(2,1)} %bitcast.83), calls=%async_computation | async-start | bytes 524288 | tf_op jit(solution)/shard_map/all_to_all | solution.py:353
  7.7 3.7 %copy-start.9 = (f32[256,1408]{1,0:T(8,128)S(1)}, f32[256,1408]{1,0:T(8,128)}, u32[]{:S(2)}) copy-start(f32[256,1408]{1,0:T(8,128)} %param.23) | copy-start | bytes 4325380
  11.5 1.6 copy-start.10
  11.5 1.6 copy-start.11
  11.5 1.6 copy-start.12
  18.5 100.3 %copy-start = (bf16[4,8,8,512]{3,2,0,1:T(8,128)(2,1)S(1)}, bf16[4,8,8,512]{3,2,0,1:T(8,128)(2,1)}, u32[]{:S(2)}) copy-start(bf16[4,8,8,512]{3,2,0,1:T(8,128)(2,1)} %copy.48) | copy-start | bytes 786436
  18.5 100.3 %copy-start.3 = (f32[2048]{0:T(1024)S(1)}, f32[2048]{0:T(1024)}, u32[]{:S(2)}) copy-start(f32[2048]{0:T(1024)} %param.38) | copy-start | bytes 24580
  18.5 100.3 %copy-start.4 = (f32[2048]{0:T(1024)S(1)}, f32[2048]{0:T(1024)}, u32[]{:S(2)}) copy-start(f32[2048]{0:T(1024)} %param.39) | copy-start | bytes 24580
  118.1 120.0 %slice-start = ((s8[8650752]{0:T(1024)(128)(4,1)}), s8[262144]{0:T(1024)(128)(4,1)S(1)}, s32[]{:S(2)}) async-start(s8[8650752]{0:T(1024)(128)(4,1)} %bitcast.59), calls=%async_computation.2 | async-start | bytes 524288
  118.8 1.6 copy-start.1
  120.4 1.2 copy-start.2
  121.6 54.3 %copy-start.5 = (f32[2048]{0:T(1024)S(1)}, f32[2048]{0:T(1024)}, u32[]{:S(2)}) copy-start(f32[2048]{0:T(1024)} %param.40) | copy-start | bytes 24580
  121.6 54.3 %copy-start.6 = (f32[2048]{0:T(1024)S(1)}, f32[2048]{0:T(1024)}, u32[]{:S(2)}) copy-start(f32[2048]{0:T(1024)} %param.41) | copy-start | bytes 24580
  121.6 116.5 %slice-start.1 = ((s8[8650752]{0:T(1024)(128)(4,1)}), s8[4194304]{0:T(1024)(128)(4,1)S(1)}, s32[]{:S(2)}) async-start(s8[8650752]{0:T(1024)(128)(4,1)} %bitcast.59), calls=%async_computation.3 | async-start | bytes 8388608
  121.6 116.5 %slice-start.2 = ((s8[8650752]{0:T(1024)(128)(4,1)}), s8[4194304]{0:T(1024)(128)(4,1)S(1)}, s32[]{:S(2)}) async-start(s8[8650752]{0:T(1024)(128)(4,1)} %bitcast.59), calls=%async_computation.4 | async-start | bytes 8388608
  175.9 62.2 %copy-start.7 = (f32[2048]{0:T(1024)S(1)}, f32[2048]{0:T(1024)}, u32[]{:S(2)}) copy-start(f32[2048]{0:T(1024)} %param.42) | copy-start | bytes 24580
  175.9 62.2 %copy-start.8 = (f32[2048]{0:T(1024)S(1)}, f32[2048]{0:T(1024)}, u32[]{:S(2)}) copy-start(f32[2048]{0:T(1024)} %param.43) | copy-start | bytes 24580

commit v3 on v2

--- a/solution.py
+++ b/solution.py
@@ -20,11 +20,12 @@
 VMEM = pl.BlockSpec(memory_space=pltpu.VMEM)
 
 
-def greet(depth, axes):
+def greet(depth, axes, others=()):
     barrier = pltpu.get_barrier_semaphore()
     z = lax.axis_index("z")
     targets = [{"z": lax.rem(z + d, depth)} for d in range(1, depth)]
     targets += [{axis: 1 - lax.axis_index(axis)} for axis in axes]
+    targets += others
     for target in targets:
         pl.semaphore_signal(barrier, inc=1, device_id=target, device_id_type=BY_AXIS)
     pl.semaphore_wait(barrier, len(targets))
@@ -50,8 +51,11 @@
     width = w_ref.shape[-1]
     greet(depth, ("y", "x", "c"))
 
-    def place(px, pz, py):
-        return block_place(g_ref, px, pz, py, width)
+    mats = w_ref.shape[1]
+
+    def place(px, pz, py, piece=slice(None)):
+        start = pl.multiple_of((pz * 2 + py) * width, width)
+        return g_ref.at[piece, px, :, pl.ds(start, width)]
 
     to_x, to_y, to_c = {"x": 1 - x}, {"y": 1 - y}, {"c": 1 - c}
     scale_sends, token_sends, z_copies, m_copies = [], [], [], []
@@ -65,19 +69,24 @@
         copy.start()
     beside = [remote(t_ref, ta_ref.at[0, c], tcsend.at[0], tcrecv.at[0], to_c)]
     beside[0].start()
-    own_y = remote(w_ref.at[z], place(x, z, y), ysend.at[0], yrecv.at[0], to_y)
-    own_x = remote(w_ref.at[z], place(x, z, y), xsend.at[0], xrecv.at[0], to_x)
-    own_y.start()
-    own_x.start()
-    y_copies, x_copies, d_copies = [own_y], [own_x], []
+    y_copies, x_copies, d_copies = [], [], []
+    for p in range(mats):
+        y_copies.append(remote(w_ref.at[z, p], place(x, z, y, p), ysend.at[p], yrecv.at[p], to_y))
+        x_copies.append(remote(w_ref.at[z, p], place(x, z, y, p), xsend.at[p], xrecv.at[p], to_x))
+        y_copies[p].start()
+        x_copies[p].start()
     for d in range(1, depth):
         target = {"z": lax.rem(z + d, depth)}
         scale_sends.append(remote(s_ref, sa_ref.at[c, x, y, z], ssend.at[d], srecv.at[d], target))
         scale_sends[-1].start()
     for d in range(1, depth):
         target = lax.rem(z + d, depth)
-        z_copies.append(remote(w_ref.at[target], place(x, z, y), zsend.at[d], zrecv.at[d], {"z": target}))
-        z_copies[-1].start()
+        for p in range(mats):
+            slot = d * mats + p
+            z_copies.append(
+                remote(w_ref.at[target, p], place(x, z, y, p), zsend.at[slot], zrecv.at[slot], {"z": target})
+            )
+            z_copies[-1].start()
     for d in range(1, depth):
         target = {"z": lax.rem(z + d, depth)}
         token_sends.append(remote(t_ref, ta_ref.at[d, c], tzsend.at[d], tzrecv.at[d], target))
@@ -87,16 +96,17 @@
         m_copies.append(remote(m_ref.at[target], held_ref.at[d], msend.at[d], mrecv.at[d], {"z": target}))
         m_copies[-1].start()
 
-    def relay(d):
+    def relay(e):
+        d, p = divmod(e, mats)
         source = lax.rem(z - d + depth, depth)
-        if d % 2 == 0:
-            y_copies[d].wait_recv()
-            block = place(x, source, 1 - y)
-            copy = remote(block, block, dsend.at[d], drecv.at[d], to_x)
+        if e % 2 == 0:
+            y_copies[e].wait_recv()
+            block = place(x, source, 1 - y, p)
+            copy = remote(block, block, dsend.at[e], drecv.at[e], to_x)
         else:
-            x_copies[d].wait_recv()
-            block = place(1 - x, source, y)
-            copy = remote(block, block, dsend.at[d], drecv.at[d], to_y)
+            x_copies[e].wait_recv()
+            block = place(1 - x, source, y, p)
+            copy = remote(block, block, dsend.at[e], drecv.at[e], to_y)
         copy.start()
         d_copies.append(copy)
 
@@ -109,32 +119,32 @@
         hop = remote(part, part, ssend.at[slot], srecv.at[slot], target)
         hop.start()
         hop.wait()
-    for d in range(1, depth):
-        block = place(x, lax.rem(z - d + depth, depth), y)
-        z_copies[d - 1].wait_recv()
-        ycopy = remote(block, block, ysend.at[d], yrecv.at[d], to_y)
-        xcopy = remote(block, block, xsend.at[d], xrecv.at[d], to_x)
+    count = depth * mats
+    for e in range(mats, count):
+        d, p = divmod(e, mats)
+        block = place(x, lax.rem(z - d + depth, depth), y, p)
+        z_copies[e - mats].wait_recv()
+        ycopy = remote(block, block, ysend.at[e], yrecv.at[e], to_y)
+        xcopy = remote(block, block, xsend.at[e], xrecv.at[e], to_x)
         ycopy.start()
         xcopy.start()
         y_copies.append(ycopy)
         x_copies.append(xcopy)
-        relay(d - 1)
-    relay(depth - 1)
+        relay(e - mats)
+    for e in range(count - mats, count):
+        relay(e)
     for d in range(1, depth):
         token_sends[d - 1].wait_recv()
         copy = remote(ta_ref.at[d, c], ta_ref.at[d, c], tcsend.at[d], tcrecv.at[d], to_c)
         copy.start()
         beside.append(copy)
-    for d in range(depth):
-        if d % 2 == 0:
-            x_copies[d].wait_recv()
-        else:
-            y_copies[d].wait_recv()
-        d_copies[d].wait_recv()
-        y_copies[d].wait_send()
-        x_copies[d].wait_send()
-        d_copies[d].wait_send()
-        beside[d].wait()
+    for e in range(count):
+        (x_copies if e % 2 == 0 else y_copies)[e].wait_recv()
+        d_copies[e].wait()
+        y_copies[e].wait_send()
+        x_copies[e].wait_send()
+    for copy in beside:
+        copy.wait()
     for copy in m_copies:
         copy.wait()
     for copy in z_copies + token_sends:
@@ -156,7 +166,8 @@
         ),
         in_specs=[ANY] * 4,
         out_specs=(ANY,) * 4,
-        scratch_shapes=[dma((depth,)) for _ in range(10)]
+        scratch_shapes=[dma((depth * mats,)) for _ in range(8)]
+        + [dma((depth,)), dma((depth,))]
         + [dma((depth + 2,)), dma((depth + 2,))]
         + [dma((depth,)) for _ in range(4)]
         + [dma((4,))],
@@ -195,7 +206,7 @@
     return jnp.dot(gated, merged(weights, 3), preferred_element_type=jnp.float32)
 
 
-def stage_kernel(depth, chunk, first, *refs):
+def stage_kernel(depth, chunk, first, final, *refs):
     refs = list(refs)
     take = lambda n: [refs.pop(0) for _ in range(n)]
     w_ref, f_ref, k_ref, own_ref, scale_ref, gain_ref, shift_ref = take(7)
@@ -223,7 +234,12 @@
             keeps[d].start()
     else:
         whole, zsend, zrecv, csend, crecv = take(5)
-        greet(depth, ("c",))
+        if final:
+            sheet, fsend, frecv = take(3)
+            x = lax.axis_index("x")
+            greet(depth, ("x", "c"), [{"x": 1 - x, "c": 1 - c}])
+        else:
+            greet(depth, ("c",))
         beside = remote(own_ref, whole.at[0, c], csend.at[0], crecv.at[0], to_c)
         beside.start()
         across = []
@@ -292,7 +308,23 @@
     mean_square = jnp.sum(summed * summed, -1, keepdims=True) / count
     variance = mean_square - average * average
     normed = (summed - average) * lax.rsqrt(variance + EPSILON) * gain_ref[...] + shift_ref[...]
-    out_ref[...] = normed.astype(jnp.bfloat16)
+    if final:
+        rows, columns = own_ref.shape[0], out_ref.shape[1]
+        own_place = x * CORES + c
+        here = pl.ds(pl.multiple_of(own_place * rows, rows), rows)
+        sheet[...] = normed.astype(jnp.bfloat16)
+        leaving = []
+        for k, (tx, tc) in enumerate(((1 - x, c), (1 - x, 1 - c), (x, 1 - c))):
+            there = pl.ds(pl.multiple_of((tx * CORES + tc) * columns, columns), columns)
+            leaving.append(
+                remote(sheet.at[:, there], out_ref.at[here], fsend.at[k], frecv.at[k], {"x": tx, "c": tc})
+            )
+            leaving[-1].start()
+        out_ref[here] = sheet[:, pl.ds(pl.multiple_of(own_place * columns, columns), columns)]
+        for copy in leaving:
+            copy.wait()
+    else:
+        out_ref[...] = normed.astype(jnp.bfloat16)
     for d in range(depth):
         handover(d).wait_send()
         if d > 0:
@@ -311,7 +343,7 @@
             across[d - 1].wait_send()
 
 
-def stage(depth, number, chunk, weights, factors, taps, own, scale, gain, shift, whole=None, held=None):
+def stage(depth, number, chunk, weights, factors, taps, own, scale, gain, shift, whole=None, held=None, final=False):
     rows, features = own.shape
     first = whole is not None
     dma = pltpu.SemaphoreType.DMA
@@ -331,8 +363,11 @@
         scratch += [dma((depth,)) for _ in range(7)]
     else:
         scratch += [pair] + [dma((depth,)) for _ in range(4)]
+    if final:
+        out_shape = [jax.ShapeDtypeStruct((2 * CORES * rows, features // (2 * CORES)), jnp.bfloat16)]
+        scratch += [pltpu.VMEM((rows, features), jnp.bfloat16), dma((3,)), dma((3,))]
     return pl.pallas_call(
-        functools.partial(stage_kernel, depth, chunk, first),
+        functools.partial(stage_kernel, depth, chunk, first, final),
         out_shape=tuple(out_shape),
         in_specs=in_specs,
         out_specs=tuple(out_specs),
@@ -390,9 +425,9 @@
         depth, 2, mixer_chunk, mixer_weights, mixer_factors, taps, first, mixout_cols, mixer_gain, mixer_shift
     )
     (last,) = stage(
-        depth, 3, feed_chunk, feed_weights, feed_factors, taps, second, down_cols, last_gain, last_shift
-    )
-    return lax.all_to_all(last, ("x", "c"), 1, 0, tiled=True)
+        depth, 3, feed_chunk, feed_weights, feed_factors, taps, second, down_cols, last_gain, last_shift, final=True
+    )
+    return last
 
 
 def add_rows(gathered, shard_piece):

time: 304 us -> 285 us (0.938)
  Pallas kernels: 271 us -> 261 us
  blocking collectives: 8.39 us -> 0 us
    pallas_call x3, Pallas kernels: 173 us -> 162 us  [stage(): pl.pallas_call(functools.partial(stage_kernel, depth, chunk, first, final...]
    all_to_all x1 -> x0, blocking collectives: 8.39 us -> none  [column_plan(): return lax.all_to_all(last, ('x', 'c'), 1, 0, tiled=True)]
  transfers between devices with their start and end apart: 1 -> 1, of which waited for: 0 -> 0; matrix products, arithmetic and copies ran while one was open for 4% -> 5% of each run, Pallas kernels for 0% -> 0%
where the time goes in v3:
time: 285 us
  Pallas kernels  261 us (92%)
  local copies, waits for them, and re-layouts  11.4 us (4%)
  other arithmetic  8 us (3%)
  starting transfers between devices  4.37 us (2%)
    pallas_call x3, Pallas kernels, stage(): pl.pallas_call(functools.partial(stage_kernel, depth, chunk, first, final...  162 us
    pallas_call x1, Pallas kernels, spread_weights(): pl.pallas_call(functools.partial(weights_kernel, depth), out_shape=(jax.S...  98.4 us
  transfers between devices with their start and end apart: 1, of which 0 were waited for; matrix products, arithmetic and copies ran while one was open for 5% of the time, Pallas kernels for 0%

profile of v3, /device:TPU:0, one launch (start us, length us, event | category | flops | bytes accessed | tf_op | source)
XLA Modules:
  0.0 284.9 jit_solution(2087080414463070443)
XLA Ops:
  0.0 4.4 %all-to-all-start = ((bf16[4,64,512]{2,1,0:T(8,128)(2,1)}), bf16[4,64,512]{2,1,0:T(8,128)(2,1)S(1)}, u32[]{:S(2)}, u32[]{:S(2)}) async-start(bf16[4,64,512]{2,1,0:T(8,128)(2,1)} %bitcast.73), calls=%async_computation | async-start | bytes 524288 | tf_op jit(solution)/shard_map/all_to_all | solution.py:388
  4.4 0.8 concatenate.3
  5.2 0.6 pad_bitcast_fusion.s_ref
  5.8 0.8 reshape.63
  6.6 1.1 convert_bitcast_fusion.4
  7.7 0.0 copy-start.9
  7.7 0.8 copy.34
  8.5 0.0 copy-done.13
  8.6 0.9 copy.35
  9.4 0.0 copy-done.14
  9.4 0.8 copy.36
  10.3 1.1 convert_element_type.49
  11.4 0.0 copy-done.9
  11.4 0.1 convert_bitcast_fusion.1
  11.5 0.0 copy-start.10
  11.5 0.0 copy-start.11
  11.5 0.0 copy-start.12
  11.5 1.5 convert_bitcast_fusion
  13.0 0.0 copy-done.10
  13.0 1.1 pad_maximum_fusion.1.m_ref
  14.2 0.3 copy.32
  14.4 0.3 copy.33
  14.7 1.4 convert_element_type.42
  16.2 1.6 pad_maximum_fusion.w_ref
  17.7 0.0 all-to-all-done
  17.7 0.7 copy.45
  18.5 98.4 %spread_weights.1 = (bf16[3,2,352,2048]{3,2,1,0:T(8,128)(2,1)}, bf16[4,4,128,256]{3,2,1,0:T(8,128)(2,1)}, f32[2,2,2,4,8,128]{5,4,3,2,1,0:T(8,128)}, bf16[4,2,64,2048]{3,2,1,0:T(8,128)(2,1)}) custom-call(bf16[4,3,352,256]{3,2,1,0:T(8,128)(2,1)} %pad_maximum_fusion.w_ref, bf16[4,4,128,256]{3,2,1,0:T(8,128)(2,1)} %pad_maximum_fusion.1.m_ref, ...), custom_call_target="tpu_custom_call" | custom-call | tf_op jit(solution)/shard_map/spread_weights/pallas_call | solution.py:159
  116.9 0.9 reshape.62
  117.9 0.1 fusion
  118.0 0.1 fusion.1
  118.1 0.1 fusion.2
  118.2 0.1 mul.22.refs_4_
  118.3 0.1 stack_reshape.43
  118.3 0.1 stack_reshape.45
  118.4 0.1 stack_reshape.47
  118.5 0.1 stack_reshape.46
  118.6 0.1 stack_reshape.44
  118.7 0.1 broadcast_in_dim_reshape.3.refs_4_
  118.8 1.6 copy-done.1
  120.4 1.2 copy-done.2
  121.7 42.5 %stage_1.1 = (bf16[64,2048]{1,0:T(8,128)(2,1)S(1)}, bf16[4,2,128,2048]{3,2,1,0:T(8,128)(2,1)S(1)}) custom-call(bf16[3,2,352,2048]{3,2,1,0:T(8,128)(2,1)} %get-tuple-element.11.refs_0_, f32[2,704]{1,0:T(2,128)S(1)} %pad_maximum_fusion.2.refs_1_, f32[3,256]{1,0:T(4,128)S(1)} %bitcast.56, bf16[64,2048]{1,0:T(8,128)(2,1)S(1)} %bitcast.55, ...), custom_call_target="tpu_custom_call" | custom-call | tf_op jit(solution)/shard_map/stage_1/pallas_call | solution.py:369
  164.1 0.0 copy-done.5
  164.1 0.0 copy-done.6
  164.1 0.0 copy-start.7
  164.2 0.0 copy-start.8
  164.2 60.2 %stage_2.1.refs_3_ = bf16[64,2048]{1,0:T(8,128)(2,1)S(1)} custom-call(bf16[4,2,128,2048]{3,2,1,0:T(8,128)(2,1)S(1)} %get-tuple-element.15.refs_0_, f32[3,256]{1,0:T(4,128)S(1)} %pad_maximum_fusion.3.refs_1_, f32[3,256]{1,0:T(4,128)S(1)} %bitcast.57, bf16[64,2048]{1,0:T(8,128)(2,1)S(1)} %get-tuple-element.16.refs_3_, ...), custom_call_target="tpu_custom_call" | custom-call | tf_op jit(solution)/shard_map/stage_2/pallas_call | solution.py:369
  224.4 59.8 %stage_3.1 = bf16[256,512]{1,0:T(8,128)(2,1)S(1)} custom-call(bf16[3,2,352,2048]{3,2,1,0:T(8,128)(2,1)S(1)} %bitcast.53, f32[2,704]{1,0:T(2,128)S(1)} %pad_maximum_fusion.2.refs_1_, f32[3,256]{1,0:T(4,128)S(1)} %bitcast.58, bf16[64,2048]{1,0:T(8,128)(2,1)S(1)} %stage_2.1.refs_3_, f32[1,2048]{1,0:T(1,128)S(1)} %mul.22.refs_4_, f32[1,2048]{1,0:T(1,128)S(1)} %bitcast.63, ...), custom_call_target="tpu_custom_call" | custom-call | tf_op jit(solution)/shard_map/stage_3/pallas_call | solution.py:369
  284.2 0.7 copy.55
  (32 shorter events, 0.2 us)
Async XLA Ops:
  0.0 8.5 %copy-start.13 = (f32[256,512]{1,0:T(8,128)S(1)}, f32[256,512]{1,0:T(8,128)}, u32[]{:S(2)}) copy-start(f32[256,512]{1,0:T(8,128)} %param.30) | copy-start | bytes 1572868
  0.0 9.4 %copy-start.14 = (f32[256,512]{1,0:T(8,128)S(1)}, f32[256,512]{1,0:T(8,128)}, u32[]{:S(2)}) copy-start(f32[256,512]{1,0:T(8,128)} %param.31) | copy-start | bytes 1572868
  0.0 17.7 %all-to-all-start = ((bf16[4,64,512]{2,1,0:T(8,128)(2,1)}), bf16[4,64,512]{2,1,0:T(8,128)(2,1)S(1)}, u32[]{:S(2)}, u32[]{:S(2)}) async-start(bf16[4,64,512]{2,1,0:T(8,128)(2,1)} %bitcast.73), calls=%async_computation | async-start | bytes 524288 | tf_op jit(solution)/shard_map/all_to_all | solution.py:388
  7.7 3.7 %copy-start.9 = (f32[256,1408]{1,0:T(8,128)S(1)}, f32[256,1408]{1,0:T(8,128)}, u32[]{:S(2)}) copy-start(f32[256,1408]{1,0:T(8,128)} %param.23) | copy-start | bytes 4325380
  11.5 1.6 copy-start.10
  11.5 1.6 copy-start.11
  11.5 1.6 copy-start.12
  18.5 100.3 %copy-start = (bf16[4,8,8,512]{3,2,0,1:T(8,128)(2,1)S(1)}, bf16[4,8,8,512]{3,2,0,1:T(8,128)(2,1)}, u32[]{:S(2)}) copy-start(bf16[4,8,8,512]{3,2,0,1:T(8,128)(2,1)} %copy.45) | copy-start | bytes 786436
  18.5 100.3 %copy-start.3 = (f32[2048]{0:T(1024)S(1)}, f32[2048]{0:T(1024)}, u32[]{:S(2)}) copy-start(f32[2048]{0:T(1024)} %param.38) | copy-start | bytes 24580
  18.5 100.3 %copy-start.4 = (f32[2048]{0:T(1024)S(1)}, f32[2048]{0:T(1024)}, u32[]{:S(2)}) copy-start(f32[2048]{0:T(1024)} %param.39) | copy-start | bytes 24580
  118.1 106.2 %slice-start = ((s8[8650752]{0:T(1024)(128)(4,1)}), s8[262144]{0:T(1024)(128)(4,1)S(1)}, s32[]{:S(2)}) async-start(s8[8650752]{0:T(1024)(128)(4,1)} %bitcast.52), calls=%async_computation.1 | async-start | bytes 524288
  118.8 1.6 copy-start.1
  120.4 1.2 copy-start.2
  121.6 42.5 %copy-start.5 = (f32[2048]{0:T(1024)S(1)}, f32[2048]{0:T(1024)}, u32[]{:S(2)}) copy-start(f32[2048]{0:T(1024)} %param.40) | copy-start | bytes 24580
  121.6 42.5 %copy-start.6 = (f32[2048]{0:T(1024)S(1)}, f32[2048]{0:T(1024)}, u32[]{:S(2)}) copy-start(f32[2048]{0:T(1024)} %param.41) | copy-start | bytes 24580
  121.6 102.7 %slice-start.1 = ((s8[8650752]{0:T(1024)(128)(4,1)}), s8[4194304]{0:T(1024)(128)(4,1)S(1)}, s32[]{:S(2)}) async-start(s8[8650752]{0:T(1024)(128)(4,1)} %bitcast.52), calls=%async_computation.2 | async-start | bytes 8388608
  121.6 102.7 %slice-start.2 = ((s8[8650752]{0:T(1024)(128)(4,1)}), s8[4194304]{0:T(1024)(128)(4,1)S(1)}, s32[]{:S(2)}) async-start(s8[8650752]{0:T(1024)(128)(4,1)} %bitcast.52), calls=%async_computation.3 | async-start | bytes 8388608
  164.1 60.3 %copy-start.7 = (f32[2048]{0:T(1024)S(1)}, f32[2048]{0:T(1024)}, u32[]{:S(2)}) copy-start(f32[2048]{0:T(1024)} %param.42) | copy-start | bytes 24580
  164.2 60.3 %copy-start.8 = (f32[2048]{0:T(1024)S(1)}, f32[2048]{0:T(1024)}, u32[]{:S(2)}) copy-start(f32[2048]{0:T(1024)} %param.43) | copy-start | bytes 24580
